TPU v7x, 256 devices: a whole 4x4x8 slice. The times are simulated.
256 devices in a mesh: sp: 64 (over z, y, core), tp: 4 (over x).
Axes of the slice: x: 4, y: 4, z: 8, core: 2. Of those that a mesh axis runs over, the one named last changes fastest.
Arguments:
- residual: bfloat16 [49152, 2048], P(('sp', 'tp')), may hold values from -6 to 6
- queries: bfloat16 [49152, 1024], P('sp', 'tp'), may hold values from -240 to 240
- keys: bfloat16 [49152, 256], P('sp', 'tp'), may hold values from -6 to 6
- values: bfloat16 [49152, 256], P('sp', 'tp'), may hold values from -18 to 18
- sinks: float32 [16], P('tp'), may hold values from 1 to 6
- out_weight: bfloat16 [1024, 2048], replicated, may hold values from -0.5625 to 0.5625
- norm_gain: float32 [2048], replicated, may hold values from 0.1 to 1.9
- gate_weight: bfloat16 [2048, 5632], P('sp', 'tp'), may hold values from -0.125 to 0.125
- up_weight: bfloat16 [2048, 5632], P('sp', 'tp'), may hold values from -0.125 to 0.125
- down_weight: bfloat16 [5632, 2048], P('tp', 'sp'), may hold values from -0.078125 to 0.078125
Outputs:
- layer_out: bfloat16 [49152, 2048], P(('sp', 'tp'))
All inputs are finite; a program needn't handle non-finite values.
Results may differ from a plain program's by a relative error of at most 0.014.
Values may be sent and summed in bfloat16 or wider, within the bound.
A program may use at most 128 MiB of HBM per device.

v0:
```python
import jax
import jax.numpy as jnp
from jax import lax
from jax.sharding import PartitionSpec as P

HEAD = 64
WINDOW = 128


def turned_gather(arrays, axis, dims):
    turned = [jnp.moveaxis(a, dim, 0) for a, dim in zip(arrays, dims)]
    both = jnp.concatenate([t.reshape(len(t), -1) for t in turned], axis=1)
    filled, at, done = (lax.all_gather(both, axis, axis=0, tiled=True), 0, [])
    for t, dim in zip(turned, dims):
        piece = filled[:, at : at + t[0].size].reshape(-1, *t.shape[1:])
        done.append(jnp.moveaxis(piece, 0, dim))
        at += t[0].size
    return tuple(done)


def passed_along(block, axis, distance):
    devices = range(lax.axis_size(axis))
    route = [(i - distance, i) for i in devices if i - distance in devices]
    return lax.ppermute(block, axis, route)


def copy_for_each(x, axis):
    size = lax.axis_size(axis)
    return lax.all_to_all(jnp.broadcast_to(x[None], (size, *x.shape)), axis, 0, 0, tiled=True)


def joined_along(tiles, dim):
    tiles = jnp.moveaxis(tiles, 0, dim)
    dims = tiles.shape
    return tiles.reshape(*dims[:dim], dims[dim] * dims[dim + 1], *dims[dim + 2 :])


def gather_directly(x, axis, dim):
    tiles = copy_for_each(x, axis)
    return joined_along(tiles, dim)


def attend(queries, keys_ext, values_ext, sinks, block_base):
    rows = queries.shape[0]
    nblk = rows // WINDOW
    qheads = sinks.shape[0]
    kheads = keys_ext.shape[1] // HEAD
    group = qheads // kheads
    qblock = queries.reshape(nblk, WINDOW, kheads, group, HEAD).astype(jnp.float32)

    def band(arr):
        first = arr[:rows].reshape(nblk, WINDOW, kheads, HEAD)
        second = arr[WINDOW:].reshape(nblk, WINDOW, kheads, HEAD)
        return jnp.concatenate([first, second], axis=1).astype(jnp.float32)

    kband = band(keys_ext)
    vband = band(values_ext)
    score = jnp.einsum("nqhgd,nkhd->nhgqk", qblock, kband) * HEAD ** (-0.5)
    qidx = jnp.arange(WINDOW)[:, None]
    kidx = jnp.arange(2 * WINDOW)[None, :]
    rel = qidx + WINDOW - kidx
    valid = (rel >= 0) & (rel < WINDOW)
    blocks = block_base + jnp.arange(nblk)
    valid = valid[None] & ((blocks > 0)[:, None, None] | (kidx >= WINDOW)[None])
    score = jnp.where(valid[:, None, None], score, -jnp.inf)
    sink = sinks.reshape(kheads, group)[None, :, :, None]
    top = jnp.maximum(jnp.max(score, axis=-1), sink)
    expd = jnp.exp(score - top[..., None])
    denom = jnp.sum(expd, axis=-1) + jnp.exp(sink - top)
    weights = (expd / denom[..., None]).astype(jnp.bfloat16)
    result = jnp.einsum("nhgqk,nkhd->nqhgd", weights.astype(jnp.float32), vband)
    return result.reshape(rows, qheads * HEAD).astype(jnp.bfloat16)


def shards(
    residual,
    queries,
    keys,
    values,
    sinks,
    out_weight,
    norm_gain,
    gate_weight,
    up_weight,
    down_weight,
):
    rows_dev = queries.shape[0]
    gate_whole, up_whole, down_whole = turned_gather(
        (gate_weight, up_weight, down_weight), "sp", (0, 0, 1)
    )
    prev_keys, prev_values = passed_along((keys[-WINDOW:], values[-WINDOW:]), "sp", 1)
    keys_ext = jnp.concatenate([prev_keys, keys], axis=0)
    values_ext = jnp.concatenate([prev_values, values], axis=0)
    attention = attend(
        queries, keys_ext, values_ext, sinks, lax.axis_index("sp") * (rows_dev // WINDOW)
    )
    head_rows = lax.all_to_all(attention, "tp", split_axis=0, concat_axis=1, tiled=True)
    proj = jnp.dot(head_rows, out_weight, preferred_element_type=jnp.float32)
    mixed = (residual.astype(jnp.float32) + proj).astype(jnp.bfloat16)
    mixf = mixed.astype(jnp.float32)
    normed = (
        mixf * lax.rsqrt(jnp.mean(mixf * mixf, axis=-1, keepdims=True) + 1e-06) * norm_gain
    ).astype(jnp.bfloat16)
    normed_all = gather_directly(normed, "tp", 0)
    gate = jnp.dot(normed_all, gate_whole, preferred_element_type=jnp.float32)
    upper = jnp.dot(normed_all, up_whole, preferred_element_type=jnp.float32)
    hidden = (jax.nn.silu(gate) * upper).astype(jnp.bfloat16)
    ffn = lax.psum_scatter(
        jnp.dot(hidden, down_whole, preferred_element_type=jnp.float32).astype(jnp.bfloat16),
        "tp",
        scatter_dimension=0,
        tiled=True,
    ).astype(jnp.float32)
    return (mixed.astype(jnp.float32) + ffn).astype(jnp.bfloat16)


def solution(mesh):
    placed = (
        P(("sp", "tp"), None),
        P("sp", "tp"),
        P("sp", "tp"),
        P("sp", "tp"),
        P("tp"),
        P(),
        P(),
        P("sp", "tp"),
        P("sp", "tp"),
        P("tp", "sp"),
    )
    return jax.shard_map(
        shards, mesh=mesh, in_specs=placed, out_specs=P(("sp", "tp"), None), check_vma=False
    )
```

profile of v0, /device:TPU:1, one launch (start us, length us, event | category | flops | bytes accessed | tf_op | source)
XLA Modules:
  0.0 189.2 jit_solution(14304794351753541043)
XLA Ops:
  6.5 1.7 pad_maximum_fusion
  8.3 0.0 all-gather.2.cloned.1.call-update
  8.3 0.0 reduce-scatter.2.cloned.1.call-start
  8.4 0.7 slice.21
  9.1 4.6 %collective-permute-start = (bf16[128,64]{0,1:T(8,128)(2,1)S(1)}, bf16[128,64]{0,1:T(8,128)(2,1)S(1)}, u32[]{:S(2)}, u32[]{:S(2)}) collective-permute-start(bf16[128,64]{0,1:T(8,128)(2,1)S(1)} %slice.21), channel_id=1, source_target_pairs={{0,4},{4,8},{8,12},{12,16},{16,20},{20,24},{24,28},{28,32},{32,36}... | collective-permute-start | bytes 49160 | tf_op jit(solution)/shard_map/ppermute | solution.py:24
  13.7 0.7 slice.23
  14.4 1.9 %collective-permute-start.1 = (bf16[128,64]{0,1:T(8,128)(2,1)S(1)}, bf16[128,64]{0,1:T(8,128)(2,1)S(1)}, u32[]{:S(2)}, u32[]{:S(2)}) collective-permute-start(bf16[128,64]{0,1:T(8,128)(2,1)S(1)} %slice.23), channel_id=1, source_target_pairs={{0,4},{4,8},{8,12},{12,16},{16,20},{20,24},{24,28},{28,32},{32,36}... | collective-permute-start | bytes 49160 | tf_op jit(solution)/shard_map/ppermute | solution.py:24
  16.3 0.1 broadcast_or_fusion
  16.5 0.3 broadcast_and_fusion
  16.7 1.0 reshape.153
  17.8 1.0 reshape.150
  18.8 1.8 reshape.160
  20.7 0.1 reshape.152
  20.9 0.1 reshape.149
  21.1 0.7 fusion.14
  21.9 0.1 broadcast_maximum_fusion
  21.9 0.7 fusion.11
  22.7 0.1 exponential_add_fusion
  22.7 0.9 fusion.23
  23.7 0.6 copy.37
  24.3 0.5 reshape.161
  24.8 10.9 %all_to_all.21 = bf16[4,192,256]{2,1,0:T(8,128)(2,1)S(1)} all-to-all(bf16[4,192,256]{2,1,0:T(8,128)(2,1)S(1)} %reshape.161), channel_id=1, replica_groups=mesh['sp'=64,'tp'=4] {'tp'}, dimensions={0} | all-to-all | bytes 786432 | tf_op jit(solution)/shard_map/all_to_all | solution.py:97
  35.7 3.4 %multiply_reduce_fusion = (f32[192]{0:T(256)S(1)}, f32[192,2048]{1,0:T(8,128)S(1)}) fusion(bf16[192,1024]{1,0:T(8,128)(2,1)S(1)} %bitcast.63, bf16[1024,2048]{1,0:T(8,128)(2,1)} %param.15, bf16[192,2048]{1,0:T(8,128)(2,1)S(1)} %copy-done), kind=kOutput, calls=%fused_computation.20 | convolution fusion | flops 807665472 | bytes 6947584 | tf_op jit(solution)/shard_map/dot_general | solution.py:98
  39.1 0.2 multiply_convert_fusion.1
  39.3 0.4 broadcast_in_dim.16
  39.7 39.1 %all_to_all.22 = bf16[4,192,2048]{2,1,0:T(8,128)(2,1)} all-to-all(bf16[4,192,2048]{2,1,0:T(8,128)(2,1)S(1)} %broadcast_in_dim.16), channel_id=1, replica_groups=mesh['sp'=64,'tp'=4] {'tp'}, dimensions={0} | all-to-all | bytes 6291456 | tf_op jit(solution)/shard_map/all_to_all | solution.py:29
  78.8 36.0 %all-gather.2.cloned.1.call-done = bf16[2048,4224]{1,0:T(8,128)(2,1)} async-done(((bf16[32,4224]{1,0:T(8,128)(2,1)}), bf16[2048,4224]{1,0:T(8,128)(2,1)}) %all-gather.2.cloned.1.call-update) | async-done | bytes 17301520 | tf_op jit(solution)/shard_map/all_gather | solution.py:13
  114.8 9.7 %fusion.4 = f32[768,1408]{1,0:T(8,128)} fusion(bf16[768,2048]{1,0:T(8,128)(2,1)} %bitcast.61, bf16[2048,4224]{1,0:T(8,128)(2,1)} %all-gather.2.cloned.1.call-done), kind=kOutput, calls=%fused_computation.4 | convolution fusion | flops 4429185024 | bytes 13238272 | tf_op jit(solution)/shard_map/dot_general | solution.py:105
  124.5 18.2 %fusion.8 = bf16[768,2048]{1,0:T(8,128)(2,1)} fusion(bf16[2048,4224]{1,0:T(8,128)(2,1)} %all-gather.2.cloned.1.call-done, f32[768,1408]{1,0:T(8,128)} %fusion.4, bf16[768,2048]{1,0:T(8,128)(2,1)} %bitcast.62), kind=kOutput, calls=%fused_computation.7 | convolution fusion | flops 8866430976 | bytes 22151168 | tf_op jit(solution)/shard_map/dot_general | solution.py:109
  142.7 0.0 reduce-scatter.2.cloned.1.call-update
  142.7 37.5 %reduce-scatter.2.cloned.1.call-done = bf16[192,2048]{1,0:T(8,128)(2,1)} async-done(((bf16[768,2048]{1,0:T(8,128)(2,1)}), bf16[192,2048]{1,0:T(8,128)(2,1)}) %reduce-scatter.2.cloned.1.call-update) | async-done | bytes 786448 | tf_op jit(solution)/shard_map/reduce_scatter | solution.py:108
  180.2 2.2 %add_convert_fusion = bf16[192,2048]{1,0:T(8,128)(2,1)} fusion(f32[192,2048]{1,0:T(8,128)S(1)} %get-tuple-element.8, bf16[192,2048]{1,0:T(8,128)(2,1)} %reduce-scatter.2.cloned.1.call-done), kind=kLoop, calls=%fused_computation.18 | loop fusion | flops 1179648 | bytes 3145728 | tf_op jit(solution)/shard_map/convert_element_type | solution.py:114
  (25 shorter events, 0.2 us)
Async XLA Ops:
  6.5 14.4 %copy-start.2 = (bf16[768,64]{0,1:T(8,128)(2,1)S(1)}, bf16[768,64]{0,1:T(8,128)(2,1)}, u32[]{:S(2)}) copy-start(bf16[768,64]{0,1:T(8,128)(2,1)} %param.13) | copy-start | bytes 294916
  6.5 14.2 %copy-start.1 = (bf16[768,64]{0,1:T(8,128)(2,1)S(1)}, bf16[768,64]{0,1:T(8,128)(2,1)}, u32[]{:S(2)}) copy-start(bf16[768,64]{0,1:T(8,128)(2,1)} %param.12) | copy-start | bytes 294916
  6.5 108.3 %all-gather.2.cloned.1.call-start = ((), (), s32[]{:S(2)}) async-start(), calls=%async_computation.3 | async-start | bytes 17571840 | tf_op jit(solution)/shard_map/all_gather | solution.py:13
  8.3 171.9 %reduce-scatter.2.cloned.1.call-start = ((), (), s32[]{:S(2)}) async-start(), calls=%async_computation.4 | async-start | bytes 3932160 | tf_op jit(solution)/shard_map/reduce_scatter | solution.py:108
  9.1 11.8 %collective-permute-start = (bf16[128,64]{0,1:T(8,128)(2,1)S(1)}, bf16[128,64]{0,1:T(8,128)(2,1)S(1)}, u32[]{:S(2)}, u32[]{:S(2)}) collective-permute-start(bf16[128,64]{0,1:T(8,128)(2,1)S(1)} %slice.21), channel_id=1, source_target_pairs={{0,4},{4,8},{8,12},{12,16},{16,20},{20,24},{24,28},{28,32},{32,36}... | collective-permute-start | bytes 49160 | tf_op jit(solution)/shard_map/ppermute | solution.py:24
  14.4 6.3 %collective-permute-start.1 = (bf16[128,64]{0,1:T(8,128)(2,1)S(1)}, bf16[128,64]{0,1:T(8,128)(2,1)S(1)}, u32[]{:S(2)}, u32[]{:S(2)}) collective-permute-start(bf16[128,64]{0,1:T(8,128)(2,1)S(1)} %slice.23), channel_id=1, source_target_pairs={{0,4},{4,8},{8,12},{12,16},{16,20},{20,24},{24,28},{28,32},{32,36}... | collective-permute-start | bytes 49160 | tf_op jit(solution)/shard_map/ppermute | solution.py:24
  20.7 1.2 copy-start.4
  23.7 12.0 %copy-start = (bf16[192,2048]{1,0:T(8,128)(2,1)S(1)}, bf16[192,2048]{1,0:T(8,128)(2,1)}, u32[]{:S(2)}) copy-start(bf16[192,2048]{1,0:T(8,128)(2,1)} %param.10) | copy-start | bytes 2359300
  35.7 3.4 %copy-start.3 = (f32[2048]{0:T(1024)S(1)}, f32[2048]{0:T(1024)}, u32[]{:S(2)}) copy-start(f32[2048]{0:T(1024)} %param.16) | copy-start | bytes 24580
Sparse Core Ops, SparseCore 0:
  10.1 104.7 all-gather.1
  142.8 37.3 reduce-scatter.1
where the time goes:
time: 190 us; the launch traced here: 189 us
  waiting for transfers between devices  73.5 us (39%)
  blocking collectives  50 us (26%)
  matrix products  32.9 us (17%)
  between operations  13.7 us (7%)
  local copies, waits for them, and re-layouts  7.15 us (4%)
  starting transfers between devices  6.52 us (3%)
  other arithmetic  5.46 us (3%)
    all_to_all x1, blocking collectives, copy_for_each(): lax.all_to_all(jnp.broadcast_to(x[None], (size, *x.shape)), axis, 0, 0, t...  39.1 us
    reduce_scatter x1, waiting for transfers between devices, shards(): lax.psum_scatter(jnp.dot(hidden, down_whole, preferred_element_type=jnp.f...  37.5 us
    all_gather x1, waiting for transfers between devices, turned_gather(): filled, at, done = (lax.all_gather(both, axis, axis=0, tiled=True), 0, [])  36 us
    dot_general x1, matrix products, shards(): jnp.dot(hidden, down_whole, preferred_element_type=jnp.float32)  18.2 us
    all_to_all x1, blocking collectives, shards(): lax.all_to_all(attention, 'tp', split_axis=0, concat_axis=1, tiled=True)  10.9 us
    dot_general x1, matrix products, shards(): gate = jnp.dot(normed_all, gate_whole, preferred_element_type=jnp.float32)  9.67 us
    ppermute x2, starting transfers between devices, passed_along(): return lax.ppermute(block, axis, route)  6.48 us
  transfers between devices with their start and end apart: 4, of which 2 were waited for; matrix products, arithmetic and copies ran while one was open for 7% of the time, Pallas kernels for 0%

commit v1 on v0

v1 whole, which is shorter than its diff:
```python
import functools

import jax
import jax.numpy as jnp
from jax import lax
from jax.experimental import pallas as pl
from jax.experimental.pallas import tpu as pltpu
from jax.sharding import PartitionSpec as P

MESH = pl.DeviceIdType.MESH
BF16, F32 = jnp.bfloat16, jnp.float32
HEAD = 64
WINDOW = 128
NZ, NY, NC, NX = 8, 4, 2, 4
ROWS = 768
MINE = 192
D, FFD = 2048, 1408
GA = 4
DA = 640
NT = (((1,), (1,)), ((), ()))
LABELS = (0, -1, 1, -2, 2, -3, 3, -4)
PER = 57


def kernel(
    res_h, q_h, k_h, v_h, sink_s, wo_h, gain_h, g_h, u_h, d_h, out_h,
    gu, dt, xs, hid, ao, at, wo, res, mix, qv, kx, vx, gain, draw,
    sa, sm, sp_, ra, rfm, rfp, own, outv,
    load_sem, out_sem, gs, gr, ds_, dr, as_, ar, xsend, xrecv, rsend, rrecv, hsem,
):
    sp = lax.axis_index("sp")
    x = lax.axis_index("tp")
    z, y, c = sp // (NY * NC), (sp // NC) % NY, sp % NC
    s = 1 - 2 * c

    def spidx(zz, yy, cc):
        return (zz * NY + yy) * NC + cc

    def zat(k):
        return (z + k * s + NZ) % NZ

    def yat(k):
        return (y + k * s + NY) % NY

    def xat(k):
        return (x + k * s + NX) % NX

    to_yp = {"sp": spidx(z, yat(1), c)}
    to_ym = {"sp": spidx(z, yat(-1), c)}
    to_zp = {"sp": spidx(zat(1), y, c)}
    to_zm = {"sp": spidx(zat(-1), y, c)}
    to_core = {"sp": spidx(z, y, 1 - c)}
    to_xp = {"tp": xat(1)}
    to_xm = {"tp": xat(-1)}
    nsp = NZ * NY * NC
    to_next = {"sp": (sp + 1) % nsp}
    to_prev = {"sp": (sp + nsp - 1) % nsp}

    def load(src, dst, i):
        pltpu.make_async_copy(src, dst, load_sem.at[i]).start()

    def loaded(dst, i):
        pltpu.make_async_copy(dst, dst, load_sem.at[i]).wait()

    for n in range(11):
        load(g_h.at[:, pl.ds(128 * n, 128)], gu.at[n, z, y, c, :, pl.ds(0, 128)], 0)
        load(u_h.at[:, pl.ds(128 * n, 128)], gu.at[n, z, y, c, :, pl.ds(128, 128)], 0)
    load(k_h, kx.at[pl.ds(WINDOW, ROWS)], 1)
    load(v_h, vx.at[pl.ds(WINDOW, ROWS)], 2)
    load(q_h, qv, 3)
    load(d_h, draw, 4)
    for n in range(8):
        load(wo_h.at[:, pl.ds(256 * n, 256)], wo.at[n], 5)
        load(res_h.at[:, pl.ds(256 * n, 256)], res.at[n], 6)
    load(gain_h, gain, 7)

    barrier = pltpu.get_barrier_semaphore()
    peers = [to_yp, to_ym, to_zp, to_zm, to_core, to_next, to_prev]
    peers += [{"tp": (x + j) % NX} for j in (1, 2, 3)]
    for peer in peers:
        pl.semaphore_signal(barrier, inc=1, device_id=peer, device_id_type=MESH)
    pl.semaphore_wait(barrier, len(peers))

    def remote(src, dst, send, recv, to):
        return pltpu.make_async_remote_copy(
            src_ref=src, dst_ref=dst, send_sem=send, recv_sem=recv, device_id=to, device_id_type=MESH
        )

    ALL = slice(None)

    def gu_at(part, zz, yy, cc):
        tiles = pl.ds(0, GA) if part == "a" else pl.ds(GA, 11 - GA)
        return gu.at[tiles, zz, yy, cc]

    def dt_at(part, zz, yy, cc):
        lanes = pl.ds(0, DA) if part == "a" else pl.ds(DA, FFD - DA)
        return dt.at[zz, yy, cc, :, lanes]

    def stream(view, send_sem, recv_sem):
        slots = {}

        def slot(key):
            return slots.setdefault(key, len(slots))

        sent = []

        def send(key, part, zz, yy, to):
            i = slot(key)
            copy = remote(
                view(part, zz, yy, c), view(part, zz, yy, c), send_sem.at[i], recv_sem.at[i], to
            )
            copy.start()
            sent.append(copy)

        def recv(key, part, zz, yy, cc=None):
            i = slot(key)
            ref = view(part, zz, yy, c if cc is None else cc)
            remote(ref, ref, send_sem.at[i], recv_sem.at[i], to_core).wait_recv()

        def start():
            send("ay-1", "a", z, y, to_yp)
            send("ay+1", "a", z, y, to_ym)
            send("bz-1", "b", z, y, to_zp)
            send("bz+1", "b", z, y, to_zm)
            by_out(0)

        def by_out(k):
            send(f"by-1,{k}", "b", zat(k), y, to_yp)
            send(f"by+1,{k}", "b", zat(k), y, to_ym)

        def a_y1():
            recv("ay-1", "a", z, yat(-1))
            send("ay-2", "a", z, yat(-1), to_yp)
            recv("ay+1", "a", z, yat(1))

        def a_y2():
            recv("ay-2", "a", z, yat(-2))
            send("az-1", "a", z, ALL, to_zp)
            send("az+1", "a", z, ALL, to_zm)
            send("ad0", "a", z, ALL, to_core)

        def a_z(k):
            recv(f"az{k:+d}", "a", zat(k), ALL)
            if -4 < k < 0:
                send(f"az{k - 1:+d}", "a", zat(k), ALL, to_zp)
            if 0 < k < 3:
                send(f"az{k + 1:+d}", "a", zat(k), ALL, to_zm)
            send(f"ad{k}", "a", zat(k), ALL, to_core)

        def b_z(k):
            recv(f"bz{k:+d}", "b", zat(k), y)
            if -4 < k < 0:
                send(f"bz{k - 1:+d}", "b", zat(k), y, to_zp)
            if 0 < k < 3:
                send(f"bz{k + 1:+d}", "b", zat(k), y, to_zm)
            by_out(k)

        def b_y1(k):
            recv(f"by-1,{k}", "b", zat(k), yat(-1))
            send(f"by-2,{k}", "b", zat(k), yat(-1), to_yp)
            recv(f"by+1,{k}", "b", zat(k), yat(1))

        def b_y2(k):
            recv(f"by-2,{k}", "b", zat(k), yat(-2))
            send(f"bd{k}", "b", zat(k), ALL, to_core)

        def partner(part, k):
            zz = (z - k * s + NZ) % NZ
            recv(f"{part}d{k}", part, zz, ALL, 1 - c)

        f = functools.partial
        events = [
            f(a_y1),
            f(b_z, -1), f(b_z, 1),
            f(a_y2),
            f(b_y1, 0),
            f(b_z, -2), f(b_z, 2),
            f(b_y2, 0),
            f(a_z, -1), f(a_z, 1),
            f(b_y1, -1), f(b_y1, 1),
            f(b_z, -3), f(b_z, 3),
            f(b_y2, -1), f(b_y2, 1),
            f(b_z, -4),
            f(a_z, -2), f(a_z, 2),
            f(b_y1, -2), f(b_y1, 2),
            f(b_y2, -2), f(b_y2, 2),
            f(a_z, -3), f(a_z, 3),
            f(b_y1, -3), f(b_y1, 3),
            f(b_y2, -3), f(b_y2, 3),
            f(a_z, -4),
            f(b_y1, -4), f(b_y2, -4),
        ]
        last = [f(partner, p, k) for k in LABELS for p in "ab"]
        return start, events, last, sent

    gstart, gevents, glast, gsent = stream(gu_at, gs, gr)
    dstart, devents, dlast, dsent = stream(dt_at, ds_, dr)

    loaded(gu.at[:, z, y, c], 0)
    gstart()

    loaded(kx.at[pl.ds(WINDOW, ROWS)], 1)
    loaded(vx.at[pl.ds(WINDOW, ROWS)], 2)
    halo = []
    for i, buf in enumerate((kx, vx)):
        copy = remote(
            buf.at[pl.ds(ROWS, WINDOW)], buf.at[pl.ds(0, WINDOW)], hsem.at[i], hsem.at[2 + i], to_next
        )
        copy.start()
        halo.append(copy)

    loaded(qv, 3)
    sink = jnp.concatenate([jnp.full((WINDOW, 1), sink_s[h], F32) for h in range(4)], axis=0)
    qi = lax.broadcasted_iota(jnp.int32, (4 * WINDOW, 2 * WINDOW), 0) % WINDOW
    ki = lax.broadcasted_iota(jnp.int32, (4 * WINDOW, 2 * WINDOW), 1)
    rel = qi + WINDOW - ki
    inside = (rel >= 0) & (rel < WINDOW)

    def attend(b, valid):
        q = qv[pl.ds(pl.multiple_of(b * WINDOW, WINDOW), WINDOW), :]
        q = jnp.concatenate([q[:, h * HEAD : (h + 1) * HEAD] for h in range(4)], axis=0)
        band = pl.ds(pl.multiple_of(b * WINDOW, WINDOW), 2 * WINDOW)
        score = lax.dot_general(q, kx[band, :], NT, preferred_element_type=F32) * HEAD ** (-0.5)
        score = jnp.where(valid, score, -1e30)
        top = jnp.maximum(jnp.max(score, axis=-1, keepdims=True), sink)
        expd = jnp.exp(score - top)
        denom = jnp.sum(expd, axis=-1, keepdims=True) + jnp.exp(sink - top)
        weights = (expd * (1.0 / denom)).astype(BF16)
        o = jnp.dot(weights, vx[band, :], preferred_element_type=F32).astype(BF16)
        o = jnp.concatenate([o[h * WINDOW : (h + 1) * WINDOW] for h in range(4)], axis=1)
        ao[pl.ds(pl.multiple_of(b * WINDOW, WINDOW), WINDOW), :] = o

    @pl.loop(1, ROWS // WINDOW)
    def _(b):
        attend(b, inside)

    for copy in halo:
        copy.wait_recv()
    attend(0, inside & ((ki >= WINDOW) | (sp > 0)))

    asent = []
    for j in (1, 2, 3):
        to = (x + j) % NX
        copy = remote(
            ao.at[pl.ds(pl.multiple_of(to * MINE, MINE), MINE)], at.at[x], as_.at[j], ar.at[j], {"tp": to}
        )
        copy.start()
        asent.append(copy)
    at[x] = ao[pl.ds(pl.multiple_of(x * MINE, MINE), MINE), :]

    gi = iter(gevents)
    di = iter(devents)

    def run(it, count):
        for _ in range(count):
            next(it)()

    run(gi, 3)

    for j in (1, 2, 3):
        src = (x + NX - j) % NX
        remote(at.at[src], at.at[src], as_.at[j], ar.at[j], to_xp).wait_recv()

    loaded(wo, 5)
    loaded(res, 6)
    loaded(gain, 7)
    square = jnp.zeros((MINE, 1), F32)
    for n in range(8):
        acc = res[n].astype(F32)
        proj = jnp.zeros((MINE, 256), F32)
        for i in range(NX):
            proj += jnp.dot(at[i], wo[n, 256 * i : 256 * (i + 1), :], preferred_element_type=F32)
        m = (acc + proj).astype(BF16)
        mix[n] = m
        mf = m.astype(F32)
        square += jnp.sum(mf * mf, axis=-1, keepdims=True)
    scale = lax.rsqrt(square * (1.0 / D) + 1e-06)
    for n in range(8):
        mf = mix[n].astype(F32)
        xs[x, :, 256 * n : 256 * (n + 1)] = (
            mf * scale * gain[:, 256 * n : 256 * (n + 1)]
        ).astype(BF16)

    xsent = []

    def xsend_piece(kind, j, who, to):
        piece = xs.at[who, pl.ds(48 * j, 48)]
        copy = remote(piece, piece, xsend.at[4 * kind + j], xrecv.at[4 * kind + j], to)
        copy.start()
        xsent.append(copy)

    def xrecv_piece(kind, j, who):
        piece = xs.at[who, pl.ds(48 * j, 48)]
        remote(piece, piece, xsend.at[4 * kind + j], xrecv.at[4 * kind + j], to_xp).wait_recv()

    for j in range(4):
        xsend_piece(0, j, x, to_xp)
        xsend_piece(1, j, x, to_xm)

    loaded(draw, 4)
    eye = (
        lax.broadcasted_iota(jnp.int32, (32, 32), 0) == lax.broadcasted_iota(jnp.int32, (32, 32), 1)
    ).astype(BF16)
    dt[z, y, c] = lax.dot_general(eye, draw[...], NT, preferred_element_type=F32).astype(BF16)

    for j in range(4):
        run(gi, 5)
        xrecv_piece(0, j, xat(-1))
        xsend_piece(2, j, xat(-1), to_xp)
    run(gi, 4)
    dstart()
    run(gi, len(gevents) - 27)
    run(di, 3)
    for ev in glast:
        ev()

    def hidden(who, lo, hi):
        @pl.loop(lo, hi)
        def _(n):
            w = gu[n].reshape(D, 256)
            both = jnp.dot(xs[who], w, preferred_element_type=F32)
            gate, up = both[:, :128], both[:, 128:]
            hid[who, :, pl.ds(pl.multiple_of(n * 128, 128), 128)] = (
                gate / (1.0 + jnp.exp(-gate)) * up
            ).astype(BF16)

    for j in range(4):
        xrecv_piece(1, j, xat(1))
    who_list = (x, xat(-1), xat(1), xat(2))
    for w, who in enumerate(who_list):
        if w == 3:
            for j in range(4):
                xrecv_piece(2, j, xat(2))
        hidden(who, 0, 4)
        run(di, 2)
        hidden(who, 4, 8)
        run(di, 2)
        hidden(who, 8, 11)
        run(di, 3)
    run(di, len(devents) - 31)
    for ev in dlast:
        ev()

    def partial(who, n):
        w = dt[n].reshape(256, FFD)
        return lax.dot_general(hid[who], w, NT, preferred_element_type=F32)

    def rs(buf, dst, kind, j, to):
        return remote(
            buf.at[pl.ds(2 * j, 2)], dst.at[pl.ds(2 * j, 2)],
            rsend.at[4 * kind + j], rrecv.at[4 * kind + j], to,
        )

    @pl.loop(0, 4)
    def _(j):
        for i in range(2):
            sa[2 * j + i] = partial(xat(2), 2 * j + i).astype(BF16)
        rs(sa, ra, 0, j, to_xp).start()
        for i in range(2):
            sm[2 * j + i] = partial(xat(-1), 2 * j + i).astype(BF16)
        rs(sm, rfp, 1, j, to_xm).start()

    @pl.loop(0, 8)
    def _(n):
        own[n] = partial(x, n) + mix[n].astype(F32)

    @pl.loop(0, 4)
    def _(j):
        rs(sa, ra, 0, j, to_xp).wait_recv()
        for i in range(2):
            n = 2 * j + i
            sp_[n] = (partial(xat(1), n) + ra[n].astype(F32)).astype(BF16)
        rs(sp_, rfm, 2, j, to_xp).start()

    def out_copy(n):
        return pltpu.make_async_copy(
            outv.at[n], out_h.at[:, pl.ds(pl.multiple_of(n * 256, 256), 256)], out_sem.at[n]
        )

    @pl.loop(0, 4)
    def _(j):
        rs(sm, rfp, 1, j, to_xm).wait_recv()
        rs(sp_, rfm, 2, j, to_xp).wait_recv()
        for i in range(2):
            n = 2 * j + i
            outv[n] = (own[n] + rfp[n].astype(F32) + rfm[n].astype(F32)).astype(BF16)
            out_copy(n).start()

    for copy in halo + asent + xsent + gsent + dsent:
        copy.wait_send()

    @pl.loop(0, 4)
    def _(j):
        rs(sa, ra, 0, j, to_xp).wait_send()
        rs(sm, rfp, 1, j, to_xm).wait_send()
        rs(sp_, rfm, 2, j, to_xp).wait_send()

    @pl.loop(0, 8)
    def _(n):
        out_copy(n).wait()


def shards(residual, queries, keys, values, sinks, out_weight, norm_gain, gate, up, down):
    vmem = pltpu.VMEM
    dma = pltpu.SemaphoreType.DMA
    anyspec = pl.BlockSpec(memory_space=pl.ANY)
    smem = pl.BlockSpec(memory_space=pltpu.SMEM)
    return pl.pallas_call(
        kernel,
        out_shape=jax.ShapeDtypeStruct((MINE, D), BF16),
        in_specs=[anyspec] * 4 + [smem] + [anyspec] * 5,
        out_specs=anyspec,
        scratch_shapes=[
            vmem((11, NZ, NY, NC, 32, 256), BF16),
            vmem((NZ, NY, NC, 32, FFD), BF16),
            vmem((NX, MINE, D), BF16),
            vmem((NX, MINE, FFD), BF16),
            vmem((ROWS, 256), BF16),
            vmem((NX, MINE, 256), BF16),
            vmem((8, 1024, 256), BF16),
            vmem((8, MINE, 256), BF16),
            vmem((8, MINE, 256), BF16),
            vmem((ROWS, 256), BF16),
            vmem((ROWS + WINDOW, HEAD), BF16),
            vmem((ROWS + WINDOW, HEAD), BF16),
            vmem((1, D), F32),
            vmem((FFD, 32), BF16),
        ]
        + [vmem((8, MINE, 256), BF16)] * 6
        + [
            vmem((8, MINE, 256), F32),
            vmem((8, MINE, 256), BF16),
            dma((8,)),
            dma((8,)),
            dma((PER,)), dma((PER,)), dma((PER,)), dma((PER,)),
            dma((4,)), dma((4,)),
            dma((12,)), dma((12,)),
            dma((12,)), dma((12,)),
            dma((4,)),
        ],
        compiler_params=pltpu.CompilerParams(
            collective_id=0, has_side_effects=True, vmem_limit_bytes=62 * 1024 * 1024
        ),
    )(residual, queries, keys, values, sinks, out_weight, norm_gain.reshape(1, D), gate, up, down)


def solution(mesh):
    placed = (
        P(("sp", "tp"), None),
        P("sp", "tp"),
        P("sp", "tp"),
        P("sp", "tp"),
        P("tp"),
        P(),
        P(),
        P("sp", "tp"),
        P("sp", "tp"),
        P("tp", "sp"),
    )
    return jax.shard_map(
        shards, mesh=mesh, in_specs=placed, out_specs=P(("sp", "tp"), None), check_vma=False
    )
```

time: 190 us -> 132 us (0.69)
  Pallas kernels: 0 us -> 124 us
  waiting for transfers between devices: 73.5 us -> 0 us
  blocking collectives: 50 us -> 0 us
  matrix products: 32.9 us -> 0 us
  between operations: 13.7 us -> 0.01 us
  starting transfers between devices: 6.52 us -> 0 us
  other arithmetic: 5.46 us -> 0 us
    pallas_call x0 -> x1, Pallas kernels: none -> 124 us  [shards(): pl.pallas_call(kernel, out_shape=jax.ShapeDtypeStruct((MINE, D), BF16), i...]
    all_to_all x2 -> x0, blocking collectives: 50 us -> none  [the longest x1 39.1 us: copy_for_each(): lax.all_to_all(jnp.broadcast_to(x[None], (size, *x.shape)), axis, 0, 0, t...]
    reduce_scatter x1 -> x0, waiting for transfers between devices: 37.5 us -> none  [shards(): lax.psum_scatter(jnp.dot(hidden, down_whole, preferred_element_type=jnp.f...]
    all_gather x1 -> x0, waiting for transfers between devices: 36 us -> none  [turned_gather(): filled, at, done = (lax.all_gather(both, axis, axis=0, tiled=True), 0, [])]
    dot_general x5 -> x0, matrix products: 32.9 us -> none  [the longest x1 18.2 us: shards(): jnp.dot(hidden, down_whole, preferred_element_type=jnp.float32)]
    unnamed x10 -> x4, local copies, waits for them, and re-layouts: 0.02 us -> 7.29 us
    ppermute x2 -> x0, starting transfers between devices: 6.48 us -> none  [passed_along(): return lax.ppermute(block, axis, route)]
    convert_element_type x2 -> x0, other arithmetic: 2.39 us -> none  [the longest x1 2.19 us: shards(): return (mixed.astype(jnp.float32) + ffn).astype(jnp.bfloat16)]
  transfers between devices with their start and end apart: 4 -> 0, of which waited for: 2 -> 0; matrix products, arithmetic and copies ran while one was open for 7% -> 0% of each run, Pallas kernels for 0% -> 0%
where the time goes in v1:
time: 132 us
  Pallas kernels  124 us (94%)
  local copies, waits for them, and re-layouts  7.29 us (6%)
    pallas_call x1, Pallas kernels, shards(): pl.pallas_call(kernel, out_shape=jax.ShapeDtypeStruct((MINE, D), BF16), i...  124 us
    unnamed x4, local copies, waits for them, and re-layouts  7.29 us

profile of v1, /device:TPU:1, one launch (start us, length us, event | category | flops | bytes accessed | tf_op | source)
XLA Modules:
  0.0 131.7 jit_solution(14408461600722903848)
XLA Ops:
  0.0 1.7 %copy.11.k_h = bf16[768,64]{1,0:T(8,128)(2,1)} copy(bf16[768,64]{0,1:T(8,128)(2,1)} %param.12) | data formatting | bytes 196608 | tf_op args[2]
  1.7 1.7 %copy.12.v_h = bf16[768,64]{1,0:T(8,128)(2,1)} copy(bf16[768,64]{0,1:T(8,128)(2,1)} %param.13) | data formatting | bytes 196608 | tf_op args[3]
  3.4 1.8 %copy.13.d_h = bf16[1408,32]{1,0:T(8,128)(2,1)} copy(bf16[1408,32]{0,1:T(8,128)(2,1)} %param.19) | data formatting | bytes 180224 | tf_op args[9]
  5.2 124.4 %shard_map.100 = bf16[192,2048]{1,0:T(8,128)(2,1)} custom-call(bf16[192,2048]{1,0:T(8,128)(2,1)} %res_h.1, bf16[768,256]{1,0:T(8,128)(2,1)} %q_h.1, bf16[768,64]{1,0:T(8,128)(2,1)} %copy.11.k_h, bf16[768,64]{1,0:T(8,128)(2,1)} %copy.12.v_h, f32[4]{0:T(128)} %sink_s.1, bf16[1024,2048]{1,0:T(8,128)(2,1)} %wo_h.1, f32[1,2048]{1,0:T(1,128)} %bitcast.1, ...), custom_call_target="tpu_custom_call" | custom-call | tf_op jit(solution)/shard_map/pallas_call | solution.py:408
  129.6 2.1 %copy.15 = bf16[192,2048]{1,0:T(8,128)(2,1)} copy(bf16[192,2048]{1,0:T(8,128)(2,1)} %shard_map.100) | data formatting | bytes 1572864

commit v2 on v0

v2 whole, which is shorter than its diff:
```python
import jax
import jax.numpy as jnp
from jax import lax
from jax.experimental import pallas as pl
from jax.experimental.pallas import tpu as pltpu
from jax.sharding import PartitionSpec as P

MESH = pl.DeviceIdType.MESH
BF16, F32 = jnp.bfloat16, jnp.float32
HEAD = 64
WINDOW = 128
NZ, NY, NC, NX = 8, 4, 2, 4
ROWS = 768
MINE = 192
D, FFD = 2048, 1408
GA = 4
DA = 640
NT = (((1,), (1,)), ((), ()))
LABELS = (0, -1, 1, -2, 2, -3, 3, -4)
PER = 57
EARLY = (1, 2, 3)

ORDER = (
    "gstart", "halo", "gbo0", "at4", "at5", "at0", "a2a", "gay-1", "gay+1", "gbz-1", "gbz+1", "gbo-1", "gbo1",
    "gby-1,0", "gby+1,0", "gay-2", "gao", "gad0", "oproj", "gbz-2", "gbz+2", "gbo-2", "gbo2", "gby-1,-1",
    "gby+1,-1", "gby-1,1", "gby+1,1", "gby-2,0", "gby+1,-2", "gaz-1", "dstart", "gaz+1", "gbd0", "xf0", "xm0",
    "gad-1", "gby-1,-2", "gad1", "gby+1,2", "gbz-3", "gbo-3", "gbz+3", "gbo3", "day+1", "gby-1,2", "dbz+1",
    "gby-2,-1", "xf1", "xm1", "gbd-1", "gby-2,1", "gby+1,-3", "day-1", "gaz-2", "gbd1", "dbz-1", "gaz+2", "xf2",
    "gad-2", "xm2", "gby+1,3", "gby-2,-2", "dbz+2", "gad2", "gbz-4", "gbo-4", "gby-1,-3", "gbd-2", "gby-1,3", "xf3",
    "xm3", "gby-2,2", "day-2", "gaz-3", "gby+1,-4", "xa0", "gbd2", "gby-1,-4", "dbo0", "dbo-1", "dbz-2", "dbo1",
    "dbo-2", "dbo2", "gaz+3", "dao", "gad-3", "dbz+3", "dbo3", "gby-2,-3", "xa1", "gad3", "dad0", "gby-2,3",
    "gbd-3", "xa2", "dby+1,0", "gbd3", "dby+1,-1", "gby-2,-4", "xa3", "dby+1,1", "gaz-4", "dby-1,0", "daz+1",
    "dbz-3", "dbo-3", "dby+1,-2", "gbd-4", "dby-1,-1", "gad-4", "h1,0,1", "dby+1,2", "dby-1,1", "dad1", "h1,1,2",
    "daz-1", "h1,2,3", "dby-1,-2", "dby+1,3", "h1,3,4", "dby-1,2", "dbz-4", "dbo-4", "dby+1,-3", "dad-1", "h1,4,5",
    "dby-1,3", "h1,5,6", "daz+2", "dby-1,-3", "dby-2,0", "h1,6,7", "dby-2,-1", "h1,7,8", "daz-2", "dby-2,1", "dad2",
    "h1,8,9", "dbd0", "dby+1,-4", "dby-2,-2", "dbd-1", "h1,9,10", "dby-2,2", "dad-2", "h1,10,11", "dby-1,-4",
    "dbd1", "pa0", "dby-2,-3", "dby-2,3", "dbd-2", "dbd2", "pa1", "daz+3", "h0,0,1", "daz-3", "dbd-3", "h0,1,2",
    "dby-2,-4", "dbd3", "h0,2,3", "dad3", "h0,3,4", "dad-3", "pa2", "dbd-4", "h0,4,5", "sp0", "h0,5,7", "daz-4",
    "h0,7,8", "sp1", "h0,8,10", "dad-4", "h0,10,11", "sp2", "pa3", "pm0", "pm1", "pm2", "pm3", "fin0", "sp3",
    "fin1", "fin2", "fin3",
)


def kernel(
    res_h, q_h, k_h, v_h, sink_s, wo_h, gain_h, g_h, u_h, d_h, out_h,
    gu, dt, xs, hid, ao, at, wo, res, mix, qv, kx, vx, gain, bias,
    sa, sm, sp_, ra, rfm, rfp, own, part, outv,
    load_sem, out_sem, gs, gr, ds_, dr, as_, ar, xsend, xrecv, rsend, rrecv, hsem,
):
    sp = lax.axis_index("sp")
    x = lax.axis_index("tp")
    z, y, c = sp // (NY * NC), (sp // NC) % NY, sp % NC
    s = 1 - 2 * c

    def spidx(zz, yy, cc):
        return (zz * NY + yy) * NC + cc

    def zat(k):
        return (z + k * s + NZ) % NZ

    def yat(k):
        return (y + k * s + NY) % NY

    def xat(k):
        return (x + k * s + NX) % NX

    to_yp = {"sp": spidx(z, yat(1), c)}
    to_ym = {"sp": spidx(z, yat(-1), c)}
    to_zp = {"sp": spidx(zat(1), y, c)}
    to_zm = {"sp": spidx(zat(-1), y, c)}
    to_core = {"sp": spidx(z, y, 1 - c)}
    to_xp = {"tp": xat(1)}
    to_xm = {"tp": xat(-1)}
    nsp = NZ * NY * NC
    none = sp // nsp
    to_next = {"sp": (sp + 1) % nsp}
    to_prev = {"sp": (sp + nsp - 1) % nsp}

    barrier = pltpu.get_barrier_semaphore()
    peers = [to_yp, to_ym, to_zp, to_zm, to_core, to_next, to_prev]
    peers += [{"tp": (x + j) % NX} for j in (1, 2, 3)]
    for peer in peers:
        pl.semaphore_signal(barrier, inc=1, device_id=peer, device_id_type=MESH)

    def load(src, dst, i):
        pltpu.make_async_copy(src, dst, load_sem.at[i]).start()

    def loaded(dst, i):
        pltpu.make_async_copy(dst, dst, load_sem.at[i]).wait()

    load(q_h, qv, 3)
    for half in range(2):
        load(k_h, kx.at[pl.ds(half * HEAD, HEAD), pl.ds(WINDOW, ROWS)], 1)
        load(v_h, vx.at[pl.ds(half * HEAD, HEAD), pl.ds(WINDOW, ROWS)], 2)
    for n in range(11):
        load(g_h.at[:, pl.ds(128 * n, 128)], gu.at[n, z, y, c, :, pl.ds(0, 128)], 0)
        load(u_h.at[:, pl.ds(128 * n, 128)], gu.at[n, z, y, c, :, pl.ds(128, 128)], 0)
    load(d_h, dt.at[z, y, c], 4)
    for n in range(8):
        load(wo_h.at[:, pl.ds(256 * n, 256)], wo.at[n], 5)
        load(res_h.at[:, pl.ds(256 * n, 256)], res.at[n], 6)
    load(gain_h, gain, 7)

    def remote(src, dst, send, recv, to):
        return pltpu.make_async_remote_copy(
            src_ref=src, dst_ref=dst, send_sem=send, recv_sem=recv, device_id=to, device_id_type=MESH
        )

    steps = {}
    sent = []

    def begin(copy):
        copy.start()
        sent.append(copy)

    ALL = slice(None)

    def gu_at(half, zz, yy, cc):
        tiles = pl.ds(0, GA) if half == "a" else pl.ds(GA, 11 - GA)
        return gu.at[tiles, zz, yy, cc]

    def dt_at(half, zz, yy, cc):
        lanes = pl.ds(0, DA) if half == "a" else pl.ds(DA, FFD - DA)
        return dt.at[zz, yy, cc, :, lanes]

    def stream(m, view, send_sem, recv_sem, ready):
        slots = {}

        def slot(key):
            return slots.setdefault(key, len(slots))

        def send(key, zz, yy, to):
            i = slot(key)
            ref = view(key[0], zz, yy, c)
            begin(remote(ref, ref, send_sem.at[i], recv_sem.at[i], to))

        def recv(key, zz, yy, cc):
            i = slot(key)
            ref = view(key[0], zz, yy, cc)
            remote(ref, ref, send_sem.at[i], recv_sem.at[i], to_core).wait_recv()

        def start():
            ready()
            send("ay-1", z, y, to_yp)
            send("ay+1", z, y, to_ym)
            send("bz-1", z, y, to_zp)
            send("bz+1", z, y, to_zm)

        def a_back():
            recv("ay-1", z, yat(-1), c)
            send("ay-2", z, yat(-1), to_yp)

        def a_out():
            send("az-1", z, ALL, to_zp)
            send("az+1", z, ALL, to_zm)
            send("ad0", z, ALL, to_core)

        steps[m + "start"] = start
        steps[m + "ay-1"] = a_back
        steps[m + "ay+1"] = lambda: recv("ay+1", z, yat(1), c)
        steps[m + "ay-2"] = lambda: recv("ay-2", z, yat(-2), c)
        steps[m + "ao"] = a_out

        def along_z(kind, k, yy):
            recv(f"{kind}z{k:+d}", zat(k), yy, c)
            if -4 < k < 0:
                send(f"{kind}z{k - 1:+d}", zat(k), yy, to_zp)
            if 0 < k < 3:
                send(f"{kind}z{k + 1:+d}", zat(k), yy, to_zm)
            if kind == "a":
                send(f"ad{k}", zat(k), ALL, to_core)

        def b_out(k):
            send(f"by-1,{k}", zat(k), y, to_yp)
            send(f"by+1,{k}", zat(k), y, to_ym)

        def b_back(k):
            recv(f"by-1,{k}", zat(k), yat(-1), c)
            send(f"by-2,{k}", zat(k), yat(-1), to_yp)

        def b_last(k):
            recv(f"by-2,{k}", zat(k), yat(-2), c)
            send(f"bd{k}", zat(k), ALL, to_core)

        def partner(kind, k):
            recv(f"{kind}d{k}", (z - k * s + NZ) % NZ, ALL, 1 - c)

        for k in LABELS:
            if k:
                steps[m + f"az{k:+d}"] = lambda k=k: along_z("a", k, ALL)
                steps[m + f"bz{k:+d}"] = lambda k=k: along_z("b", k, y)
            steps[m + f"bo{k}"] = lambda k=k: b_out(k)
            steps[m + f"by-1,{k}"] = lambda k=k: b_back(k)
            steps[m + f"by+1,{k}"] = lambda k=k: recv(f"by+1,{k}", zat(k), yat(1), c)
            steps[m + f"by-2,{k}"] = lambda k=k: b_last(k)
            steps[m + f"ad{k}"] = lambda k=k: partner("a", k)
            steps[m + f"bd{k}"] = lambda k=k: partner("b", k)

    stream("g", gu_at, gs, gr, lambda: loaded(gu.at[:, z, y, c], 0))
    stream("d", dt_at, ds_, dr, lambda: loaded(dt.at[z, y, c], 4))

    qi = lax.broadcasted_iota(jnp.int32, (WINDOW, 2 * WINDOW), 0)
    ki = lax.broadcasted_iota(jnp.int32, (WINDOW, 2 * WINDOW), 1)
    rel = qi + WINDOW - ki
    bias[...] = jnp.where((rel >= 0) & (rel < WINDOW), 0.0, -1e30)
    low = lax.broadcasted_iota(jnp.int32, (WINDOW, WINDOW), 1) < HEAD
    low_b = low.astype(F32).astype(BF16)
    high_b = 1 - low_b

    def attend(b, first):
        rows = pl.ds(b * WINDOW, WINDOW)
        band = pl.ds(b * WINDOW, 2 * WINDOW)
        q = [qv[rows, t * WINDOW : (t + 1) * WINDOW] for t in range(2)]
        q = jnp.concatenate([q[0] * low_b, q[0] * high_b, q[1] * low_b, q[1] * high_b], axis=0)
        score = jnp.dot(q, kx[:, band], preferred_element_type=F32)
        off = bias[...]
        if first:
            off = jnp.where((ki < WINDOW) & (sp == 0), -1e30, off)
        weights = []
        for h in range(4):
            one = score[h * WINDOW : (h + 1) * WINDOW] * HEAD ** (-0.5) + off
            top = jnp.maximum(jnp.max(one, axis=-1, keepdims=True), sink_s[h])
            expd = jnp.exp(one - top)
            denom = jnp.sum(expd, axis=-1, keepdims=True) + jnp.exp(sink_s[h] - top)
            weights.append((expd * (1.0 / denom)).astype(BF16))
        weights = jnp.concatenate(weights, axis=0)
        o = lax.dot_general(weights, vx[:, band], NT, preferred_element_type=F32)
        for t in range(2):
            even = o[2 * t * WINDOW : (2 * t + 1) * WINDOW]
            odd = o[(2 * t + 1) * WINDOW : (2 * t + 2) * WINDOW]
            ao[rows, t * WINDOW : (t + 1) * WINDOW] = jnp.where(low, even, odd).astype(BF16)

    def halo_copy(i, buf):
        return remote(
            buf.at[:, pl.ds(ROWS, WINDOW)], buf.at[:, pl.ds(0, WINDOW)], hsem.at[i], hsem.at[2 + i], to_next
        )

    def halo():
        @pl.when(sp < nsp - 1)
        def _():
            for i, buf in enumerate((kx, vx)):
                halo_copy(i, buf).start()

    def attend_first():
        @pl.when(sp > 0)
        def _():
            for i, buf in enumerate((kx, vx)):
                halo_copy(i, buf).wait_recv()

        @pl.when(sp == 0)
        def _():
            for buf in (kx, vx):
                buf[:, :WINDOW] = jnp.zeros((2 * HEAD, WINDOW), BF16)

        attend(0, True)

    steps["halo"] = halo
    steps["at0"] = attend_first
    for b in range(1, 6):
        steps[f"at{b}"] = lambda b=b: attend(b, False)

    def exchange():
        for j in (1, 2, 3):
            to = (x + j) % NX
            mine = ao.at[pl.ds(pl.multiple_of(to * MINE, MINE), MINE)]
            begin(remote(mine, at.at[x], as_.at[j], ar.at[j], {"tp": to}))
        at[x] = ao[pl.ds(pl.multiple_of(x * MINE, MINE), MINE), :]

    def rows_copy(kind, j):
        return remote(
            xs.at[(0, 0, 1)[kind], pl.ds(48 * j, 48)], xs.at[(1, 2, 3)[kind], pl.ds(48 * j, 48)],
            xsend.at[4 * kind + j], xrecv.at[4 * kind + j], (to_xp, to_xm, to_xp)[kind],
        )

    def project():
        for j in (1, 2, 3):
            src = (x + NX - j) % NX
            remote(at.at[src], at.at[src], as_.at[j], ar.at[j], to_xp).wait_recv()
        loaded(wo, 5)
        loaded(res, 6)
        loaded(gain, 7)
        square = jnp.zeros((MINE, 1), F32)
        for n in range(8):
            proj = jnp.zeros((MINE, 256), F32)
            for i in range(NX):
                proj += jnp.dot(at[i], wo[n, 256 * i : 256 * (i + 1), :], preferred_element_type=F32)
            m = (res[n].astype(F32) + proj).astype(BF16)
            mix[n] = m
            mf = m.astype(F32)
            square += jnp.sum(mf * mf, axis=-1, keepdims=True)
        scale = lax.rsqrt(square * (1.0 / D) + 1e-06)
        for n in range(8):
            at_n = slice(256 * n, 256 * (n + 1))
            xs[0, :, at_n] = (mix[n].astype(F32) * scale * gain[:, at_n]).astype(BF16)
        for j in range(4):
            begin(rows_copy(0, j))
            begin(rows_copy(1, j))

    def pass_on(j):
        rows_copy(0, j).wait_recv()
        begin(rows_copy(2, j))

    steps["a2a"] = exchange
    steps["oproj"] = project
    for j in range(4):
        steps[f"xf{j}"] = lambda j=j: pass_on(j)
        steps[f"xm{j}"] = lambda j=j: rows_copy(1, j).wait_recv()
        steps[f"xa{j}"] = lambda j=j: rows_copy(2, j).wait_recv()

    def hidden(pair, n):
        rows = xs[2 * pair : 2 * pair + 2].reshape(2 * MINE, D)
        both = jnp.dot(rows, gu[n].reshape(D, 256), preferred_element_type=F32)
        gate, up = both[:, :128], both[:, 128:]
        h = (gate / (1.0 + jnp.exp(-gate)) * up).astype(BF16).reshape(2, MINE, 128)
        at_n = pl.ds(pl.multiple_of(n * 128, 128), 128)
        hid[2 * pair : 2 * pair + 2, :, at_n] = h

    def hidden_run(pair, lo, hi):
        pl.loop(lo + none, hi + none)(lambda n: hidden(pair, n))

    def partial(pair, n):
        rows = hid[2 * pair : 2 * pair + 2].reshape(2 * MINE, FFD)
        w = dt[zat(LABELS[n])].reshape(256, FFD)
        both = lax.dot_general(rows, w, NT, preferred_element_type=F32)
        return both[:MINE], both[MINE:]

    def sum_copy(kind, j):
        two = pl.ds(2 * j, 2)
        return remote(
            (sa, sm, sp_)[kind].at[two], (ra, rfp, rfm)[kind].at[two],
            rsend.at[4 * kind + j], rrecv.at[4 * kind + j], (to_xp, to_xm, to_xp)[kind],
        )

    def far_sums(j):
        for n in (2 * j, 2 * j + 1):
            near, far = partial(1, n)
            part[n] = near
            sa[n] = far.astype(BF16)
        begin(sum_copy(0, j))

    def near_sums(j):
        for n in (2 * j, 2 * j + 1):
            mine, back = partial(0, n)
            own[n] = mine + mix[zat(LABELS[n])].astype(F32)
            sm[n] = back.astype(BF16)
        begin(sum_copy(1, j))

    def add_on(j):
        sum_copy(0, j).wait_recv()
        for n in (2 * j, 2 * j + 1):
            sp_[n] = (part[n] + ra[n].astype(F32)).astype(BF16)
        begin(sum_copy(2, j))

    def out_copy(n):
        at_n = pl.ds(pl.multiple_of(zat(LABELS[n]) * 256, 256), 256)
        return pltpu.make_async_copy(outv.at[n], out_h.at[:, at_n], out_sem.at[n])

    def finish(j):
        sum_copy(1, j).wait_recv()
        sum_copy(2, j).wait_recv()
        for n in (2 * j, 2 * j + 1):
            outv[n] = (own[n] + rfp[n].astype(F32) + rfm[n].astype(F32)).astype(BF16)
            out_copy(n).start()

    for j in range(4):
        steps[f"pa{j}"] = lambda j=j: far_sums(j)
        steps[f"pm{j}"] = lambda j=j: near_sums(j)
        steps[f"sp{j}"] = lambda j=j: add_on(j)
        steps[f"fin{j}"] = lambda j=j: finish(j)

    loaded(qv, 3)
    loaded(kx.at[:, pl.ds(WINDOW, ROWS)], 1)
    loaded(vx.at[:, pl.ds(WINDOW, ROWS)], 2)
    for b in EARLY:
        attend(b, False)
    pl.semaphore_wait(barrier, len(peers))
    for name in ORDER:
        if name[0] == "h" and name[1] in "01":
            hidden_run(*(int(v) for v in name[1:].split(",")))
        else:
            steps[name]()
    @pl.when(sp < nsp - 1)
    def _():
        for i, buf in enumerate((kx, vx)):
            halo_copy(i, buf).wait_send()

    for copy in sent:
        copy.wait_send()
    for n in range(8):
        out_copy(n).wait()


def shards(residual, queries, keys, values, sinks, out_weight, norm_gain, gate, up, down):
    vmem = pltpu.VMEM
    dma = pltpu.SemaphoreType.DMA
    anyspec = pl.BlockSpec(memory_space=pl.ANY)
    smem = pl.BlockSpec(memory_space=pltpu.SMEM)
    return pl.pallas_call(
        kernel,
        out_shape=jax.ShapeDtypeStruct((MINE, D), BF16),
        in_specs=[anyspec] * 4 + [smem] + [anyspec] * 5,
        out_specs=anyspec,
        scratch_shapes=[
            vmem((11, NZ, NY, NC, 32, 256), BF16),
            vmem((NZ, NY, NC, 32, FFD), BF16),
            vmem((NX, MINE, D), BF16),
            vmem((NX, MINE, FFD), BF16),
            vmem((ROWS, 256), BF16),
            vmem((NX, MINE, 256), BF16),
            vmem((8, 1024, 256), BF16),
            vmem((8, MINE, 256), BF16),
            vmem((8, MINE, 256), BF16),
            vmem((ROWS, 256), BF16),
            vmem((2 * HEAD, ROWS + WINDOW), BF16),
            vmem((2 * HEAD, ROWS + WINDOW), BF16),
            vmem((1, D), F32),
            vmem((WINDOW, 2 * WINDOW), F32),
        ]
        + [vmem((8, MINE, 256), BF16)] * 6
        + [
            vmem((8, MINE, 256), F32),
            vmem((8, MINE, 256), F32),
            vmem((8, MINE, 256), BF16),
            dma((8,)),
            dma((8,)),
            dma((PER,)), dma((PER,)), dma((PER,)), dma((PER,)),
            dma((4,)), dma((4,)),
            dma((12,)), dma((12,)),
            dma((12,)), dma((12,)),
            dma((4,)),
        ],
        compiler_params=pltpu.CompilerParams(
            collective_id=0, has_side_effects=True, vmem_limit_bytes=62 * 1024 * 1024
        ),
    )(residual, queries, keys.T, values.T, sinks, out_weight, norm_gain.reshape(1, D), gate, up, down.T)


def solution(mesh):
    placed = (
        P(("sp", "tp"), None),
        P("sp", "tp"),
        P("sp", "tp"),
        P("sp", "tp"),
        P("tp"),
        P(),
        P(),
        P("sp", "tp"),
        P("sp", "tp"),
        P("tp", "sp"),
    )
    return jax.shard_map(
        shards, mesh=mesh, in_specs=placed, out_specs=P(("sp", "tp"), None), check_vma=False
    )
```

time: 190 us -> 97.3 us (0.51)
  Pallas kernels: 0 us -> 95.1 us
  waiting for transfers between devices: 73.5 us -> 0 us
  blocking collectives: 50 us -> 0 us
  matrix products: 32.9 us -> 0 us
  between operations: 13.7 us -> 0.01 us
  starting transfers between devices: 6.52 us -> 0 us
  other arithmetic: 5.46 us -> 0 us
  local copies, waits for them, and re-layouts: 7.15 us -> 2.09 us
    pallas_call x0 -> x1, Pallas kernels: none -> 95.1 us  [shards(): pl.pallas_call(kernel, out_shape=jax.ShapeDtypeStruct((MINE, D), BF16), i...]
    all_to_all x2 -> x0, blocking collectives: 50 us -> none  [the longest x1 39.1 us: copy_for_each(): lax.all_to_all(jnp.broadcast_to(x[None], (size, *x.shape)), axis, 0, 0, t...]
    reduce_scatter x1 -> x0, waiting for transfers between devices: 37.5 us -> none  [shards(): lax.psum_scatter(jnp.dot(hidden, down_whole, preferred_element_type=jnp.f...]
    all_gather x1 -> x0, waiting for transfers between devices: 36 us -> none  [turned_gather(): filled, at, done = (lax.all_gather(both, axis, axis=0, tiled=True), 0, [])]
    dot_general x5 -> x0, matrix products: 32.9 us -> none  [the longest x1 18.2 us: shards(): jnp.dot(hidden, down_whole, preferred_element_type=jnp.float32)]
    ppermute x2 -> x0, starting transfers between devices: 6.48 us -> none  [passed_along(): return lax.ppermute(block, axis, route)]
    convert_element_type x2 -> x0, other arithmetic: 2.39 us -> none  [the longest x1 2.19 us: shards(): return (mixed.astype(jnp.float32) + ffn).astype(jnp.bfloat16)]
    reshape x8 -> x0, local copies, waits for them, and re-layouts: 2.38 us -> none  [the longest x4 2.08 us: band(): second = arr[WINDOW:].reshape(nblk, WINDOW, kheads, HEAD)]
  transfers between devices with their start and end apart: 4 -> 0, of which waited for: 2 -> 0; matrix products, arithmetic and copies ran while one was open for 7% -> 0% of each run, Pallas kernels for 0% -> 0%
where the time goes in v2:
time: 97.3 us; the launch traced here: 97.2 us
  Pallas kernels  95.1 us (98%)
  local copies, waits for them, and re-layouts  2.09 us (2%)
    pallas_call x1, Pallas kernels, shards(): pl.pallas_call(kernel, out_shape=jax.ShapeDtypeStruct((MINE, D), BF16), i...  95.1 us
    unnamed x1, local copies, waits for them, and re-layouts  2.09 us

profile of v2, /device:TPU:1, one launch (start us, length us, event | category | flops | bytes accessed | tf_op | source)
XLA Modules:
  0.0 97.2 jit_solution(15274571094183701849)
XLA Ops:
  0.0 95.1 %shard_map.100 = bf16[192,2048]{1,0:T(8,128)(2,1)} custom-call(bf16[192,2048]{1,0:T(8,128)(2,1)} %res_h.1, bf16[768,256]{1,0:T(8,128)(2,1)} %q_h.1, bf16[64,768]{1,0:T(8,128)(2,1)} %bitcast.4, bf16[64,768]{1,0:T(8,128)(2,1)} %bitcast.5, f32[4]{0:T(128)} %sink_s.1, bf16[1024,2048]{1,0:T(8,128)(2,1)} %wo_h.1, f32[1,2048]{1,0:T(1,128)} %bitcast.7, ...), custom_call_target="tpu_custom_call" | custom-call | tf_op jit(solution)/shard_map/pallas_call | solution.py:398
  95.1 2.1 %copy.12 = bf16[192,2048]{1,0:T(8,128)(2,1)} copy(bf16[192,2048]{1,0:T(8,128)(2,1)} %shard_map.100) | data formatting | bytes 1572864

commit v3 on v2

--- a/solution.py
+++ b/solution.py
@@ -13,31 +13,50 @@
 ROWS = 768
 MINE = 192
 D, FFD = 2048, 1408
-GA = 4
+TILES = ((0, 5, 2), (5, 11, 7))
 DA = 640
 NT = (((1,), (1,)), ((), ()))
 LABELS = (0, -1, 1, -2, 2, -3, 3, -4)
 PER = 57
-EARLY = (1, 2, 3)
-
+
+G, Q, R, W = 0, 1, 2, 3
+START, AY, AO, AZ, BZ, BO, BY, AD, BD = range(9)
+HALO, EX, AT, PROJ, XN, XF, XM, XA, HID, PA, PN, SUM, FIN = range(20, 33)
 ORDER = (
-    "gstart", "halo", "gbo0", "at4", "at5", "at0", "a2a", "gay-1", "gay+1", "gbz-1", "gbz+1", "gbo-1", "gbo1",
-    "gby-1,0", "gby+1,0", "gay-2", "gao", "gad0", "oproj", "gbz-2", "gbz+2", "gbo-2", "gbo2", "gby-1,-1",
-    "gby+1,-1", "gby-1,1", "gby+1,1", "gby-2,0", "gby+1,-2", "gaz-1", "dstart", "gaz+1", "gbd0", "xf0", "xm0",
-    "gad-1", "gby-1,-2", "gad1", "gby+1,2", "gbz-3", "gbo-3", "gbz+3", "gbo3", "day+1", "gby-1,2", "dbz+1",
-    "gby-2,-1", "xf1", "xm1", "gbd-1", "gby-2,1", "gby+1,-3", "day-1", "gaz-2", "gbd1", "dbz-1", "gaz+2", "xf2",
-    "gad-2", "xm2", "gby+1,3", "gby-2,-2", "dbz+2", "gad2", "gbz-4", "gbo-4", "gby-1,-3", "gbd-2", "gby-1,3", "xf3",
-    "xm3", "gby-2,2", "day-2", "gaz-3", "gby+1,-4", "xa0", "gbd2", "gby-1,-4", "dbo0", "dbo-1", "dbz-2", "dbo1",
-    "dbo-2", "dbo2", "gaz+3", "dao", "gad-3", "dbz+3", "dbo3", "gby-2,-3", "xa1", "gad3", "dad0", "gby-2,3",
-    "gbd-3", "xa2", "dby+1,0", "gbd3", "dby+1,-1", "gby-2,-4", "xa3", "dby+1,1", "gaz-4", "dby-1,0", "daz+1",
-    "dbz-3", "dbo-3", "dby+1,-2", "gbd-4", "dby-1,-1", "gad-4", "h1,0,1", "dby+1,2", "dby-1,1", "dad1", "h1,1,2",
-    "daz-1", "h1,2,3", "dby-1,-2", "dby+1,3", "h1,3,4", "dby-1,2", "dbz-4", "dbo-4", "dby+1,-3", "dad-1", "h1,4,5",
-    "dby-1,3", "h1,5,6", "daz+2", "dby-1,-3", "dby-2,0", "h1,6,7", "dby-2,-1", "h1,7,8", "daz-2", "dby-2,1", "dad2",
-    "h1,8,9", "dbd0", "dby+1,-4", "dby-2,-2", "dbd-1", "h1,9,10", "dby-2,2", "dad-2", "h1,10,11", "dby-1,-4",
-    "dbd1", "pa0", "dby-2,-3", "dby-2,3", "dbd-2", "dbd2", "pa1", "daz+3", "h0,0,1", "daz-3", "dbd-3", "h0,1,2",
-    "dby-2,-4", "dbd3", "h0,2,3", "dad3", "h0,3,4", "dad-3", "pa2", "dbd-4", "h0,4,5", "sp0", "h0,5,7", "daz-4",
-    "h0,7,8", "sp1", "h0,8,10", "dad-4", "h0,10,11", "sp2", "pa3", "pm0", "pm1", "pm2", "pm3", "fin0", "sp3",
-    "fin1", "fin2", "fin3",
+    (G, START), (HALO,), (G, BO, 0), (AT, 4), (EX, 2), (EX, 1), (Q, START), (Q, BO, 0), (AT, 5), (EX, 3), (AT, 0),
+    (EX, 0), (G, AY, -1), (G, AY, 1), (G, BZ, 1), (G, BO, 1), (G, BZ, -1), (G, BO, -1), (G, BY, 1, 0), (Q, BZ, -1),
+    (Q, BO, -1), (Q, AY, -1), (Q, BZ, 1), (Q, BO, 1), (Q, AY, 1), (Q, BY, 1, 0), (G, BY, -1, 0), (G, BZ, -2),
+    (G, BO, -2), (G, AY, -2), (G, AO), (G, BY, 1, 1), (PROJ,), (Q, BZ, -2), (XN, 1), (Q, BZ, 2), (Q, BO, -2),
+    (Q, BO, 2), (G, AD, 0), (G, BY, 1, -1), (G, BY, -1, 1), (G, BY, -1, -1), (Q, BY, 1, -1), (G, BZ, -3),
+    (Q, BY, 1, 1), (Q, AY, -2), (Q, AO), (G, BY, 1, -2), (G, AZ, 1), (Q, BY, -1, 1), (Q, AD, 0), (G, AZ, -1),
+    (Q, BY, 1, -2), (G, BY, -2, 0), (G, AD, 1), (Q, BZ, 3), (Q, BO, 3), (G, AD, -1), (Q, BZ, -3), (Q, BO, -3),
+    (G, BZ, 2), (XN, 2), (Q, BY, 1, 2), (G, BD, 0), (XM, 1), (Q, BY, -1, -2), (G, BZ, -4), (G, BO, -4), (G, BO, -3),
+    (Q, BY, -1, 2), (Q, AZ, 1), (XF, 1), (Q, BY, 1, 3), (Q, AD, 1), (Q, AZ, -1), (W, START), (Q, BY, 1, -3),
+    (G, AZ, 2), (Q, AD, -1), (Q, BY, -2, 1), (G, BY, 1, -4), (G, BZ, 3), (G, BO, 3), (G, AD, 2), (G, BY, 1, -3),
+    (Q, BY, -1, 3), (G, AZ, -2), (Q, BD, 1), (XM, 2), (XF, 2), (W, AY, 1), (Q, BY, -1, -3), (Q, BZ, -4),
+    (Q, BO, -4), (G, AD, -2), (Q, BY, -2, -2), (Q, AZ, 2), (G, BY, -2, 1), (XF, 3), (G, BY, 1, 3), (G, BY, -1, -2),
+    (Q, BY, -1, -1), (Q, BD, -2), (G, BO, 2), (Q, AD, 2), (G, BD, 1), (Q, AZ, -2), (XA, 1), (XF, 0), (W, AY, -1),
+    (W, BZ, -1), (Q, BY, 1, -4), (Q, AD, -2), (G, BY, -1, 3), (G, AZ, 3), (XA, 2), (G, BY, 1, 2), (G, AD, 3),
+    (Q, BY, -2, -3), (G, AZ, -3), (Q, BY, -1, 0), (Q, BY, -1, -4), (W, BO, 0), (W, BO, -1), (Q, AZ, 3), (XA, 3),
+    (G, BY, -2, -2), (Q, BD, -3), (G, AD, -3), (XN, 0), (Q, BY, -2, -1), (W, BZ, 1), (Q, AZ, -3), (W, BO, 1),
+    (G, BY, -1, -4), (Q, AD, 3), (G, BY, -1, 2), (G, BD, -2), (W, AY, -2), (W, AO), (Q, BY, -2, 3), (XA, 0),
+    (Q, BD, -1), (G, BY, -2, 3), (Q, AD, -3), (Q, BY, -2, 2), (G, AZ, -4), (W, BY, 1, 0), (W, AD, 0), (Q, BD, 3),
+    (Q, BY, -2, 0), (G, BY, -1, -3), (G, BD, 3), (W, BY, 1, -1), (W, BZ, 2), (Q, BD, 2), (W, BO, 2), (G, AD, -4),
+    (HID, 2, 2, 0, 1), (Q, BY, -2, -4), (W, BY, 1, 1), (HID, 2, 2, 1, 2), (W, BY, -1, 0), (Q, BD, 0),
+    (G, BY, -2, -1), (XM, 0), (Q, AZ, -4), (W, BY, -1, -1), (W, BY, -1, 1), (Q, BD, -4), (HID, 2, 2, 9, 11),
+    (Q, AD, -4), (W, AZ, 1), (G, BY, -2, -4), (W, BY, 1, 2), (G, BD, -1), (HID, 2, 2, 6, 7), (W, BZ, -2),
+    (W, BZ, 3), (G, BY, -2, -3), (W, BO, -2), (G, BY, -2, 2), (W, BO, 3), (HID, 2, 2, 5, 6), (W, AZ, -1),
+    (W, AD, 1), (G, BD, -4), (W, BY, -1, 2), (HID, 2, 2, 7, 8), (G, BD, -3), (W, BY, -2, -1), (W, BY, -2, 0),
+    (HID, 2, 2, 8, 9), (G, BD, 2), (HID, 2, 2, 2, 3), (W, AD, -1), (W, BY, -2, 1), (HID, 2, 2, 3, 4), (W, BZ, -3),
+    (W, BD, -1), (W, BY, -1, -2), (W, BD, 0), (W, BO, -3), (W, BY, 1, -2), (XN, 3), (HID, 2, 2, 4, 5), (W, AZ, 2),
+    (W, BD, 1), (PA, 0), (W, BY, 1, 3), (W, BY, -1, 3), (W, BY, -2, 2), (W, AZ, -2), (W, AD, 2), (W, BZ, -4),
+    (W, BO, -4), (W, BD, 2), (W, BY, -2, -2), (PA, 1), (W, BY, -1, -3), (W, BY, 1, -3), (W, AD, -2), (W, BY, -2, 3),
+    (W, BD, -2), (XM, 3), (HID, 0, 2, 1, 2), (W, AZ, 3), (HID, 0, 2, 0, 1), (W, BY, 1, -4), (W, BY, -1, -4),
+    (W, BD, 3), (HID, 0, 2, 10, 11), (W, BY, -2, -3), (W, AZ, -3), (W, AD, 3), (PA, 2), (HID, 0, 2, 3, 4),
+    (W, BD, -3), (HID, 0, 2, 7, 8), (W, AD, -3), (HID, 0, 2, 9, 10), (W, BY, -2, -4), (HID, 0, 2, 5, 6),
+    (HID, 0, 2, 2, 3), (HID, 0, 2, 8, 9), (W, AZ, -4), (W, BD, -4), (HID, 0, 2, 4, 5), (HID, 0, 2, 6, 7), (PN, 0),
+    (W, AD, -4), (PA, 3), (SUM, 0), (PN, 1), (SUM, 1), (PN, 2), (SUM, 2), (PN, 3), (SUM, 3), (FIN, 0), (FIN, 1),
+    (FIN, 2), (FIN, 3),
 )
 
 
@@ -45,7 +64,7 @@
     res_h, q_h, k_h, v_h, sink_s, wo_h, gain_h, g_h, u_h, d_h, out_h,
     gu, dt, xs, hid, ao, at, wo, res, mix, qv, kx, vx, gain, bias,
     sa, sm, sp_, ra, rfm, rfp, own, part, outv,
-    load_sem, out_sem, gs, gr, ds_, dr, as_, ar, xsend, xrecv, rsend, rrecv, hsem,
+    load_sem, out_sem, gus, gur, ds_, dr, as_, ar, xsend, xrecv, rsend, rrecv, hsem,
 ):
     sp = lax.axis_index("sp")
     x = lax.axis_index("tp")
@@ -88,13 +107,13 @@
     def loaded(dst, i):
         pltpu.make_async_copy(dst, dst, load_sem.at[i]).wait()
 
+    for n in range(11):
+        load(g_h.at[:, pl.ds(128 * n, 128)], gu.at[n, z, y, c, :, pl.ds(0, 128)], 0)
+        load(u_h.at[:, pl.ds(128 * n, 128)], gu.at[n, z, y, c, :, pl.ds(128, 128)], 0)
     load(q_h, qv, 3)
     for half in range(2):
         load(k_h, kx.at[pl.ds(half * HEAD, HEAD), pl.ds(WINDOW, ROWS)], 1)
         load(v_h, vx.at[pl.ds(half * HEAD, HEAD), pl.ds(WINDOW, ROWS)], 2)
-    for n in range(11):
-        load(g_h.at[:, pl.ds(128 * n, 128)], gu.at[n, z, y, c, :, pl.ds(0, 128)], 0)
-        load(u_h.at[:, pl.ds(128 * n, 128)], gu.at[n, z, y, c, :, pl.ds(128, 128)], 0)
     load(d_h, dt.at[z, y, c], 4)
     for n in range(8):
         load(wo_h.at[:, pl.ds(256 * n, 256)], wo.at[n], 5)
@@ -115,12 +134,15 @@
 
     ALL = slice(None)
 
-    def gu_at(half, zz, yy, cc):
-        tiles = pl.ds(0, GA) if half == "a" else pl.ds(GA, 11 - GA)
-        return gu.at[tiles, zz, yy, cc]
+    def gu_at(first, split, last):
+        def at(half, zz, yy, cc):
+            tiles = pl.ds(first, split - first) if half == 0 else pl.ds(split, last - split)
+            return gu.at[tiles, zz, yy, cc]
+
+        return at
 
     def dt_at(half, zz, yy, cc):
-        lanes = pl.ds(0, DA) if half == "a" else pl.ds(DA, FFD - DA)
+        lanes = pl.ds(0, DA) if half == 0 else pl.ds(DA, FFD - DA)
         return dt.at[zz, yy, cc, :, lanes]
 
     def stream(m, view, send_sem, recv_sem, ready):
@@ -141,63 +163,58 @@
 
         def start():
             ready()
-            send("ay-1", z, y, to_yp)
-            send("ay+1", z, y, to_ym)
-            send("bz-1", z, y, to_zp)
-            send("bz+1", z, y, to_zm)
-
-        def a_back():
-            recv("ay-1", z, yat(-1), c)
-            send("ay-2", z, yat(-1), to_yp)
+            send((0, AY, -1), z, y, to_yp)
+            send((0, AY, 1), z, y, to_ym)
+            send((1, BZ, -1), z, y, to_zp)
+            send((1, BZ, 1), z, y, to_zm)
+
+        def a_y(k):
+            recv((0, AY, k), z, yat(k), c)
+            if k == -1:
+                send((0, AY, -2), z, yat(-1), to_yp)
 
         def a_out():
-            send("az-1", z, ALL, to_zp)
-            send("az+1", z, ALL, to_zm)
-            send("ad0", z, ALL, to_core)
-
-        steps[m + "start"] = start
-        steps[m + "ay-1"] = a_back
-        steps[m + "ay+1"] = lambda: recv("ay+1", z, yat(1), c)
-        steps[m + "ay-2"] = lambda: recv("ay-2", z, yat(-2), c)
-        steps[m + "ao"] = a_out
-
-        def along_z(kind, k, yy):
-            recv(f"{kind}z{k:+d}", zat(k), yy, c)
+            send((0, AZ, -1), z, ALL, to_zp)
+            send((0, AZ, 1), z, ALL, to_zm)
+            send((0, AD, 0), z, ALL, to_core)
+
+        def along_z(half, kind, k, yy):
+            recv((half, kind, k), zat(k), yy, c)
             if -4 < k < 0:
-                send(f"{kind}z{k - 1:+d}", zat(k), yy, to_zp)
+                send((half, kind, k - 1), zat(k), yy, to_zp)
             if 0 < k < 3:
-                send(f"{kind}z{k + 1:+d}", zat(k), yy, to_zm)
-            if kind == "a":
-                send(f"ad{k}", zat(k), ALL, to_core)
+                send((half, kind, k + 1), zat(k), yy, to_zm)
+            if half == 0:
+                send((0, AD, k), zat(k), ALL, to_core)
 
         def b_out(k):
-            send(f"by-1,{k}", zat(k), y, to_yp)
-            send(f"by+1,{k}", zat(k), y, to_ym)
-
-        def b_back(k):
-            recv(f"by-1,{k}", zat(k), yat(-1), c)
-            send(f"by-2,{k}", zat(k), yat(-1), to_yp)
-
-        def b_last(k):
-            recv(f"by-2,{k}", zat(k), yat(-2), c)
-            send(f"bd{k}", zat(k), ALL, to_core)
-
-        def partner(kind, k):
-            recv(f"{kind}d{k}", (z - k * s + NZ) % NZ, ALL, 1 - c)
-
-        for k in LABELS:
-            if k:
-                steps[m + f"az{k:+d}"] = lambda k=k: along_z("a", k, ALL)
-                steps[m + f"bz{k:+d}"] = lambda k=k: along_z("b", k, y)
-            steps[m + f"bo{k}"] = lambda k=k: b_out(k)
-            steps[m + f"by-1,{k}"] = lambda k=k: b_back(k)
-            steps[m + f"by+1,{k}"] = lambda k=k: recv(f"by+1,{k}", zat(k), yat(1), c)
-            steps[m + f"by-2,{k}"] = lambda k=k: b_last(k)
-            steps[m + f"ad{k}"] = lambda k=k: partner("a", k)
-            steps[m + f"bd{k}"] = lambda k=k: partner("b", k)
-
-    stream("g", gu_at, gs, gr, lambda: loaded(gu.at[:, z, y, c], 0))
-    stream("d", dt_at, ds_, dr, lambda: loaded(dt.at[z, y, c], 4))
+            send((1, BY, -1, k), zat(k), y, to_yp)
+            send((1, BY, 1, k), zat(k), y, to_ym)
+
+        def b_y(u, k):
+            recv((1, BY, u, k), zat(k), yat(u), c)
+            if u == -1:
+                send((1, BY, -2, k), zat(k), yat(-1), to_yp)
+            if u == -2:
+                send((1, BD, k), zat(k), ALL, to_core)
+
+        def partner(half, kind, k):
+            recv((half, kind, k), (z - k * s + NZ) % NZ, ALL, 1 - c)
+
+        steps[(m, START)] = start
+        steps[(m, AO)] = a_out
+        steps[(m, AY)] = a_y
+        steps[(m, AZ)] = lambda k: along_z(0, AZ, k, ALL)
+        steps[(m, BZ)] = lambda k: along_z(1, BZ, k, y)
+        steps[(m, BO)] = b_out
+        steps[(m, BY)] = b_y
+        steps[(m, AD)] = lambda k: partner(0, AD, k)
+        steps[(m, BD)] = lambda k: partner(1, BD, k)
+
+    for i, (m, (first, last, split)) in enumerate(zip((G, Q, R), TILES)):
+        ready = (lambda: None) if i else (lambda: loaded(gu.at[:, z, y, c], 0))
+        stream(m, gu_at(first, split, last), gus.at[i], gur.at[i], ready)
+    stream(W, dt_at, ds_, dr, lambda: loaded(dt.at[z, y, c], 4))
 
     qi = lax.broadcasted_iota(jnp.int32, (WINDOW, 2 * WINDOW), 0)
     ki = lax.broadcasted_iota(jnp.int32, (WINDOW, 2 * WINDOW), 1)
@@ -254,28 +271,32 @@
 
         attend(0, True)
 
-    steps["halo"] = halo
-    steps["at0"] = attend_first
-    for b in range(1, 6):
-        steps[f"at{b}"] = lambda b=b: attend(b, False)
-
-    def exchange():
-        for j in (1, 2, 3):
-            to = (x + j) % NX
-            mine = ao.at[pl.ds(pl.multiple_of(to * MINE, MINE), MINE)]
-            begin(remote(mine, at.at[x], as_.at[j], ar.at[j], {"tp": to}))
-        at[x] = ao[pl.ds(pl.multiple_of(x * MINE, MINE), MINE), :]
+    steps[HALO] = halo
+    steps[AT] = lambda b: attend(b, False) if b else attend_first()
+
+    def exchange_copy(to):
+        return remote(ao.at[pl.ds(to * MINE, MINE)], at.at[x], as_.at[to], ar.at[x], {"tp": to})
+
+    def exchange(to):
+        @pl.when(x != to)
+        def _():
+            exchange_copy(to).start()
+
+    def exchanged(src):
+        @pl.when(x != src)
+        def _():
+            remote(at.at[src], at.at[src], as_.at[src], ar.at[src], to_xp).wait_recv()
 
     def rows_copy(kind, j):
         return remote(
-            xs.at[(0, 0, 1)[kind], pl.ds(48 * j, 48)], xs.at[(1, 2, 3)[kind], pl.ds(48 * j, 48)],
+            xs.at[(0, 0, 2)[kind], pl.ds(48 * j, 48)], xs.at[(2, 1, 3)[kind], pl.ds(48 * j, 48)],
             xsend.at[4 * kind + j], xrecv.at[4 * kind + j], (to_xp, to_xm, to_xp)[kind],
         )
 
     def project():
-        for j in (1, 2, 3):
-            src = (x + NX - j) % NX
-            remote(at.at[src], at.at[src], as_.at[j], ar.at[j], to_xp).wait_recv()
+        at[x] = ao[pl.ds(pl.multiple_of(x * MINE, MINE), MINE), :]
+        for j in range(NX):
+            exchanged(j)
         loaded(wo, 5)
         loaded(res, 6)
         loaded(gain, 7)
@@ -294,32 +315,31 @@
             xs[0, :, at_n] = (mix[n].astype(F32) * scale * gain[:, at_n]).astype(BF16)
         for j in range(4):
             begin(rows_copy(0, j))
-            begin(rows_copy(1, j))
 
     def pass_on(j):
         rows_copy(0, j).wait_recv()
         begin(rows_copy(2, j))
 
-    steps["a2a"] = exchange
-    steps["oproj"] = project
-    for j in range(4):
-        steps[f"xf{j}"] = lambda j=j: pass_on(j)
-        steps[f"xm{j}"] = lambda j=j: rows_copy(1, j).wait_recv()
-        steps[f"xa{j}"] = lambda j=j: rows_copy(2, j).wait_recv()
-
-    def hidden(pair, n):
-        rows = xs[2 * pair : 2 * pair + 2].reshape(2 * MINE, D)
-        both = jnp.dot(rows, gu[n].reshape(D, 256), preferred_element_type=F32)
-        gate, up = both[:, :128], both[:, 128:]
-        h = (gate / (1.0 + jnp.exp(-gate)) * up).astype(BF16).reshape(2, MINE, 128)
-        at_n = pl.ds(pl.multiple_of(n * 128, 128), 128)
-        hid[2 * pair : 2 * pair + 2, :, at_n] = h
-
-    def hidden_run(pair, lo, hi):
-        pl.loop(lo + none, hi + none)(lambda n: hidden(pair, n))
-
-    def partial(pair, n):
-        rows = hid[2 * pair : 2 * pair + 2].reshape(2 * MINE, FFD)
+    steps[EX] = exchange
+    steps[PROJ] = project
+    steps[XF] = pass_on
+    steps[XN] = lambda j: begin(rows_copy(1, j))
+    steps[XM] = lambda j: rows_copy(1, j).wait_recv()
+    steps[XA] = lambda j: rows_copy(2, j).wait_recv()
+
+    def hidden(lo, count, first, last):
+        @pl.loop(first + none, last + none)
+        def _(n):
+            rows = xs[lo : lo + count].reshape(count * MINE, D)
+            both = jnp.dot(rows, gu[n].reshape(D, 256), preferred_element_type=F32)
+            gate, up = both[:, :128], both[:, 128:]
+            h = (gate / (1.0 + jnp.exp(-gate)) * up).astype(BF16)
+            hid[lo : lo + count, :, pl.ds(pl.multiple_of(n * 128, 128), 128)] = h.reshape(count, MINE, 128)
+
+    steps[HID] = hidden
+
+    def partial(lo, count, n):
+        rows = hid[lo : lo + count].reshape(count * MINE, FFD)
         w = dt[zat(LABELS[n])].reshape(256, FFD)
         both = lax.dot_general(rows, w, NT, preferred_element_type=F32)
         return both[:MINE], both[MINE:]
@@ -331,19 +351,19 @@
             rsend.at[4 * kind + j], rrecv.at[4 * kind + j], (to_xp, to_xm, to_xp)[kind],
         )
 
-    def far_sums(j):
+    def sums_out(j):
         for n in (2 * j, 2 * j + 1):
-            near, far = partial(1, n)
-            part[n] = near
+            back, far = partial(2, 2, n)
             sa[n] = far.astype(BF16)
+            sm[n] = back.astype(BF16)
         begin(sum_copy(0, j))
-
-    def near_sums(j):
+        begin(sum_copy(1, j))
+
+    def sums_kept(j):
         for n in (2 * j, 2 * j + 1):
-            mine, back = partial(0, n)
+            mine, ahead = partial(0, 2, n)
             own[n] = mine + mix[zat(LABELS[n])].astype(F32)
-            sm[n] = back.astype(BF16)
-        begin(sum_copy(1, j))
+            part[n] = ahead
 
     def add_on(j):
         sum_copy(0, j).wait_recv()
@@ -362,27 +382,32 @@
             outv[n] = (own[n] + rfp[n].astype(F32) + rfm[n].astype(F32)).astype(BF16)
             out_copy(n).start()
 
-    for j in range(4):
-        steps[f"pa{j}"] = lambda j=j: far_sums(j)
-        steps[f"pm{j}"] = lambda j=j: near_sums(j)
-        steps[f"sp{j}"] = lambda j=j: add_on(j)
-        steps[f"fin{j}"] = lambda j=j: finish(j)
+    steps[PA] = sums_out
+    steps[PN] = sums_kept
+    steps[SUM] = add_on
+    steps[FIN] = finish
 
     loaded(qv, 3)
     loaded(kx.at[:, pl.ds(WINDOW, ROWS)], 1)
     loaded(vx.at[:, pl.ds(WINDOW, ROWS)], 2)
-    for b in EARLY:
+    for b in (1, 2, 3):
         attend(b, False)
     pl.semaphore_wait(barrier, len(peers))
     for name in ORDER:
-        if name[0] == "h" and name[1] in "01":
-            hidden_run(*(int(v) for v in name[1:].split(",")))
+        if name[0] <= W:
+            steps[name[:2]](*name[2:])
         else:
-            steps[name]()
+            steps[name[0]](*name[1:])
     @pl.when(sp < nsp - 1)
     def _():
         for i, buf in enumerate((kx, vx)):
             halo_copy(i, buf).wait_send()
+
+    for to in range(NX):
+
+        @pl.when(x != to)
+        def _(to=to):
+            exchange_copy(to).wait_send()
 
     for copy in sent:
         copy.wait_send()
@@ -423,7 +448,7 @@
             vmem((8, MINE, 256), BF16),
             dma((8,)),
             dma((8,)),
-            dma((PER,)), dma((PER,)), dma((PER,)), dma((PER,)),
+            dma((len(TILES), PER)), dma((len(TILES), PER)), dma((PER,)), dma((PER,)),
             dma((4,)), dma((4,)),
             dma((12,)), dma((12,)),
             dma((12,)), dma((12,)),

time: 97.3 us -> 92.2 us (0.948)
  Pallas kernels: 95.1 us -> 90 us
    pallas_call x1, Pallas kernels: 95.1 us -> 90 us  [shards(): pl.pallas_call(kernel, out_shape=jax.ShapeDtypeStruct((MINE, D), BF16), i...]
where the time goes in v3:
time: 92.2 us; the launch traced here: 92 us
  Pallas kernels  90 us (98%)
  local copies, waits for them, and re-layouts  2.09 us (2%)
    pallas_call x1, Pallas kernels, shards(): pl.pallas_call(kernel, out_shape=jax.ShapeDtypeStruct((MINE, D), BF16), i...  90 us
    unnamed x1, local copies, waits for them, and re-layouts  2.09 us

profile of v3, /device:TPU:1, one launch (start us, length us, event | category | flops | bytes accessed | tf_op | source)
XLA Modules:
  0.0 92.0 jit_solution(11716164008355256743)
XLA Ops:
  0.0 90.0 %shard_map.100 = bf16[192,2048]{1,0:T(8,128)(2,1)} custom-call(bf16[192,2048]{1,0:T(8,128)(2,1)} %res_h.1, bf16[768,256]{1,0:T(8,128)(2,1)} %q_h.1, bf16[64,768]{1,0:T(8,128)(2,1)} %bitcast.4, bf16[64,768]{1,0:T(8,128)(2,1)} %bitcast.5, f32[4]{0:T(128)} %sink_s.1, bf16[1024,2048]{1,0:T(8,128)(2,1)} %wo_h.1, f32[1,2048]{1,0:T(1,128)} %bitcast.7, ...), custom_call_target="tpu_custom_call" | custom-call | tf_op jit(solution)/shard_map/pallas_call | solution.py:423
  90.0 2.1 %copy.12 = bf16[192,2048]{1,0:T(8,128)(2,1)} copy(bf16[192,2048]{1,0:T(8,128)(2,1)} %shard_map.100) | data formatting | bytes 1572864

commit v4 on v3

--- a/solution.py
+++ b/solution.py
@@ -13,8 +13,8 @@
 ROWS = 768
 MINE = 192
 D, FFD = 2048, 1408
-TILES = ((0, 5, 2), (5, 11, 7))
-DA = 640
+TILES = ((0, 11, 4),)
+DA = 512
 NT = (((1,), (1,)), ((), ()))
 LABELS = (0, -1, 1, -2, 2, -3, 3, -4)
 PER = 57
@@ -23,40 +23,30 @@
 START, AY, AO, AZ, BZ, BO, BY, AD, BD = range(9)
 HALO, EX, AT, PROJ, XN, XF, XM, XA, HID, PA, PN, SUM, FIN = range(20, 33)
 ORDER = (
-    (G, START), (HALO,), (G, BO, 0), (AT, 4), (EX, 2), (EX, 1), (Q, START), (Q, BO, 0), (AT, 5), (EX, 3), (AT, 0),
-    (EX, 0), (G, AY, -1), (G, AY, 1), (G, BZ, 1), (G, BO, 1), (G, BZ, -1), (G, BO, -1), (G, BY, 1, 0), (Q, BZ, -1),
-    (Q, BO, -1), (Q, AY, -1), (Q, BZ, 1), (Q, BO, 1), (Q, AY, 1), (Q, BY, 1, 0), (G, BY, -1, 0), (G, BZ, -2),
-    (G, BO, -2), (G, AY, -2), (G, AO), (G, BY, 1, 1), (PROJ,), (Q, BZ, -2), (XN, 1), (Q, BZ, 2), (Q, BO, -2),
-    (Q, BO, 2), (G, AD, 0), (G, BY, 1, -1), (G, BY, -1, 1), (G, BY, -1, -1), (Q, BY, 1, -1), (G, BZ, -3),
-    (Q, BY, 1, 1), (Q, AY, -2), (Q, AO), (G, BY, 1, -2), (G, AZ, 1), (Q, BY, -1, 1), (Q, AD, 0), (G, AZ, -1),
-    (Q, BY, 1, -2), (G, BY, -2, 0), (G, AD, 1), (Q, BZ, 3), (Q, BO, 3), (G, AD, -1), (Q, BZ, -3), (Q, BO, -3),
-    (G, BZ, 2), (XN, 2), (Q, BY, 1, 2), (G, BD, 0), (XM, 1), (Q, BY, -1, -2), (G, BZ, -4), (G, BO, -4), (G, BO, -3),
-    (Q, BY, -1, 2), (Q, AZ, 1), (XF, 1), (Q, BY, 1, 3), (Q, AD, 1), (Q, AZ, -1), (W, START), (Q, BY, 1, -3),
-    (G, AZ, 2), (Q, AD, -1), (Q, BY, -2, 1), (G, BY, 1, -4), (G, BZ, 3), (G, BO, 3), (G, AD, 2), (G, BY, 1, -3),
-    (Q, BY, -1, 3), (G, AZ, -2), (Q, BD, 1), (XM, 2), (XF, 2), (W, AY, 1), (Q, BY, -1, -3), (Q, BZ, -4),
-    (Q, BO, -4), (G, AD, -2), (Q, BY, -2, -2), (Q, AZ, 2), (G, BY, -2, 1), (XF, 3), (G, BY, 1, 3), (G, BY, -1, -2),
-    (Q, BY, -1, -1), (Q, BD, -2), (G, BO, 2), (Q, AD, 2), (G, BD, 1), (Q, AZ, -2), (XA, 1), (XF, 0), (W, AY, -1),
-    (W, BZ, -1), (Q, BY, 1, -4), (Q, AD, -2), (G, BY, -1, 3), (G, AZ, 3), (XA, 2), (G, BY, 1, 2), (G, AD, 3),
-    (Q, BY, -2, -3), (G, AZ, -3), (Q, BY, -1, 0), (Q, BY, -1, -4), (W, BO, 0), (W, BO, -1), (Q, AZ, 3), (XA, 3),
-    (G, BY, -2, -2), (Q, BD, -3), (G, AD, -3), (XN, 0), (Q, BY, -2, -1), (W, BZ, 1), (Q, AZ, -3), (W, BO, 1),
-    (G, BY, -1, -4), (Q, AD, 3), (G, BY, -1, 2), (G, BD, -2), (W, AY, -2), (W, AO), (Q, BY, -2, 3), (XA, 0),
-    (Q, BD, -1), (G, BY, -2, 3), (Q, AD, -3), (Q, BY, -2, 2), (G, AZ, -4), (W, BY, 1, 0), (W, AD, 0), (Q, BD, 3),
-    (Q, BY, -2, 0), (G, BY, -1, -3), (G, BD, 3), (W, BY, 1, -1), (W, BZ, 2), (Q, BD, 2), (W, BO, 2), (G, AD, -4),
-    (HID, 2, 2, 0, 1), (Q, BY, -2, -4), (W, BY, 1, 1), (HID, 2, 2, 1, 2), (W, BY, -1, 0), (Q, BD, 0),
-    (G, BY, -2, -1), (XM, 0), (Q, AZ, -4), (W, BY, -1, -1), (W, BY, -1, 1), (Q, BD, -4), (HID, 2, 2, 9, 11),
-    (Q, AD, -4), (W, AZ, 1), (G, BY, -2, -4), (W, BY, 1, 2), (G, BD, -1), (HID, 2, 2, 6, 7), (W, BZ, -2),
-    (W, BZ, 3), (G, BY, -2, -3), (W, BO, -2), (G, BY, -2, 2), (W, BO, 3), (HID, 2, 2, 5, 6), (W, AZ, -1),
-    (W, AD, 1), (G, BD, -4), (W, BY, -1, 2), (HID, 2, 2, 7, 8), (G, BD, -3), (W, BY, -2, -1), (W, BY, -2, 0),
-    (HID, 2, 2, 8, 9), (G, BD, 2), (HID, 2, 2, 2, 3), (W, AD, -1), (W, BY, -2, 1), (HID, 2, 2, 3, 4), (W, BZ, -3),
-    (W, BD, -1), (W, BY, -1, -2), (W, BD, 0), (W, BO, -3), (W, BY, 1, -2), (XN, 3), (HID, 2, 2, 4, 5), (W, AZ, 2),
-    (W, BD, 1), (PA, 0), (W, BY, 1, 3), (W, BY, -1, 3), (W, BY, -2, 2), (W, AZ, -2), (W, AD, 2), (W, BZ, -4),
-    (W, BO, -4), (W, BD, 2), (W, BY, -2, -2), (PA, 1), (W, BY, -1, -3), (W, BY, 1, -3), (W, AD, -2), (W, BY, -2, 3),
-    (W, BD, -2), (XM, 3), (HID, 0, 2, 1, 2), (W, AZ, 3), (HID, 0, 2, 0, 1), (W, BY, 1, -4), (W, BY, -1, -4),
-    (W, BD, 3), (HID, 0, 2, 10, 11), (W, BY, -2, -3), (W, AZ, -3), (W, AD, 3), (PA, 2), (HID, 0, 2, 3, 4),
-    (W, BD, -3), (HID, 0, 2, 7, 8), (W, AD, -3), (HID, 0, 2, 9, 10), (W, BY, -2, -4), (HID, 0, 2, 5, 6),
-    (HID, 0, 2, 2, 3), (HID, 0, 2, 8, 9), (W, AZ, -4), (W, BD, -4), (HID, 0, 2, 4, 5), (HID, 0, 2, 6, 7), (PN, 0),
-    (W, AD, -4), (PA, 3), (SUM, 0), (PN, 1), (SUM, 1), (PN, 2), (SUM, 2), (PN, 3), (SUM, 3), (FIN, 0), (FIN, 1),
-    (FIN, 2), (FIN, 3),
+    (G, START), (HALO,), (G, BO, 0), (AT, 4), (AT, 1), (AT, 3), (EX, 2), (AT, 2), (AT, 0), (EX, 0), (AT, 5),
+    (G, AY, -1), (EX, 3), (EX, 1), (G, BZ, -1), (G, BO, -1), (G, BZ, 1), (G, BO, 1), (G, BY, -1, 0), (G, AY, -2),
+    (G, AY, 1), (G, AO), (PROJ,), (XN, 2), (G, BY, -1, -1), (G, BZ, 2), (G, BO, 2), (XN, 0), (G, BZ, -2),
+    (G, BO, -2), (G, BY, -1, 1), (G, BY, 1, 0), (G, BY, -2, 0), (G, AZ, -1), (G, AZ, 1), (W, START), (G, BY, 1, -1),
+    (G, BY, -2, -1), (XF, 0), (G, BZ, -3), (G, BO, -3), (G, BZ, 3), (G, BO, 3), (G, BY, -1, 2), (XN, 1),
+    (G, BY, -1, -2), (XF, 1), (G, BY, 1, 1), (G, BY, -2, 1), (W, AY, -1), (G, AZ, -2), (G, AZ, 2), (XF, 2),
+    (G, BY, -1, -3), (G, BZ, -4), (G, BO, -4), (G, BY, -1, 3), (W, BO, 0), (XF, 3), (XN, 3), (W, BZ, -1),
+    (W, BO, -1), (G, BY, 1, -2), (G, BY, -2, -2), (W, AY, -2), (W, AY, 1), (W, AO), (W, BZ, 1), (W, BO, 1),
+    (G, AZ, -3), (G, AZ, 3), (G, BY, 1, -3), (G, BY, -2, -3), (W, BZ, -2), (G, BY, 1, 2), (G, BY, -2, 2),
+    (G, BY, -1, -4), (W, AZ, -1), (W, AZ, 1), (G, BY, 1, 3), (G, BY, -2, 3), (W, BZ, 2), (W, BO, 2), (W, BY, -1, 0),
+    (W, BY, -1, -1), (W, BY, -1, 1), (G, BY, 1, -4), (G, BY, -2, -4), (G, AZ, -4), (W, BY, -1, 2), (W, BO, -2),
+    (W, BZ, -3), (W, BO, -3), (W, AZ, 2), (G, BD, 0), (G, BD, -1), (G, BD, 1), (XA, 0), (G, BD, -2), (XA, 1),
+    (G, BD, -3), (G, BD, 2), (XA, 2), (XA, 3), (G, BD, 3), (G, BD, -4), (HID, 2, 2, 8, 3), (W, BY, 1, -1),
+    (W, BY, -2, -1), (W, BZ, 3), (W, BO, 3), (W, BY, 1, 1), (W, BY, -2, 1), (W, BY, 1, 0), (W, BY, -2, 0),
+    (G, AD, 0), (G, AD, -1), (G, AD, 1), (G, AD, -2), (G, AD, 2), (G, AD, -3), (G, AD, 3), (G, AD, -4),
+    (HID, 2, 2, 2, 2), (HID, 2, 2, 0, 2), (W, BZ, -4), (W, BY, 1, 2), (W, BY, -2, 2), (W, BO, -4),
+    (HID, 2, 2, 4, 2), (W, BY, -1, -2), (HID, 2, 2, 6, 2), (W, BY, -1, -3), (W, AD, 0), (W, AD, 1), (W, BD, 1),
+    (W, BD, 0), (PA, 0), (W, BY, -1, 3), (W, AZ, -2), (W, AZ, 3), (XM, 2), (XM, 0), (XM, 1), (XM, 3),
+    (HID, 0, 2, 4, 2), (W, BY, -1, -4), (W, BY, 1, -2), (W, BY, -2, -2), (W, AD, -1), (W, AD, 2), (W, BD, -1),
+    (W, BD, 2), (PA, 1), (HID, 0, 2, 2, 2), (W, BY, 1, -3), (W, BY, -2, -3), (W, BY, 1, 3), (W, BY, -2, 3),
+    (HID, 0, 2, 0, 2), (W, AZ, -3), (W, BY, 1, -4), (W, BY, -2, -4), (HID, 0, 2, 6, 2), (W, AD, -2), (W, AD, 3),
+    (W, BD, -2), (W, BD, 3), (PA, 2), (HID, 0, 2, 8, 3), (PN, 2), (W, AZ, -4), (PN, 0), (SUM, 0), (PN, 1),
+    (W, AD, -3), (W, BD, -4), (W, BD, -3), (W, AD, -4), (PA, 3), (SUM, 1), (PN, 3), (SUM, 2), (FIN, 0), (SUM, 3),
+    (FIN, 1), (FIN, 2), (FIN, 3),
 )
 
 
@@ -253,6 +243,10 @@
         )
 
     def halo():
+        loaded(qv, 3)
+        loaded(kx.at[:, pl.ds(WINDOW, ROWS)], 1)
+        loaded(vx.at[:, pl.ds(WINDOW, ROWS)], 2)
+
         @pl.when(sp < nsp - 1)
         def _():
             for i, buf in enumerate((kx, vx)):
@@ -327,14 +321,16 @@
     steps[XM] = lambda j: rows_copy(1, j).wait_recv()
     steps[XA] = lambda j: rows_copy(2, j).wait_recv()
 
-    def hidden(lo, count, first, last):
-        @pl.loop(first + none, last + none)
-        def _(n):
-            rows = xs[lo : lo + count].reshape(count * MINE, D)
-            both = jnp.dot(rows, gu[n].reshape(D, 256), preferred_element_type=F32)
-            gate, up = both[:, :128], both[:, 128:]
-            h = (gate / (1.0 + jnp.exp(-gate)) * up).astype(BF16)
-            hid[lo : lo + count, :, pl.ds(pl.multiple_of(n * 128, 128), 128)] = h.reshape(count, MINE, 128)
+    def hidden(lo, count, first, width):
+        @pl.loop(first + none, first + none + 1)
+        def _(i):
+            for u in range(width):
+                n = i + u
+                rows = xs[lo : lo + count].reshape(count * MINE, D)
+                both = jnp.dot(rows, gu[n].reshape(D, 256), preferred_element_type=F32)
+                gate, up = both[:, :128], both[:, 128:]
+                h = (gate / (1.0 + jnp.exp(-gate)) * up).astype(BF16)
+                hid[lo : lo + count, :, pl.ds(pl.multiple_of(n * 128, 128), 128)] = h.reshape(count, MINE, 128)
 
     steps[HID] = hidden
 
@@ -387,11 +383,6 @@
     steps[SUM] = add_on
     steps[FIN] = finish
 
-    loaded(qv, 3)
-    loaded(kx.at[:, pl.ds(WINDOW, ROWS)], 1)
-    loaded(vx.at[:, pl.ds(WINDOW, ROWS)], 2)
-    for b in (1, 2, 3):
-        attend(b, False)
     pl.semaphore_wait(barrier, len(peers))
     for name in ORDER:
         if name[0] <= W:

time: 92.2 us -> 90.6 us (0.983)
  Pallas kernels: 90 us -> 88.4 us
    pallas_call x1, Pallas kernels: 90 us -> 88.4 us  [shards(): pl.pallas_call(kernel, out_shape=jax.ShapeDtypeStruct((MINE, D), BF16), i...]
where the time goes in v4:
time: 90.6 us; the launch traced here: 90.5 us
  Pallas kernels  88.4 us (98%)
  local copies, waits for them, and re-layouts  2.09 us (2%)
    pallas_call x1, Pallas kernels, shards(): pl.pallas_call(kernel, out_shape=jax.ShapeDtypeStruct((MINE, D), BF16), i...  88.4 us
    unnamed x1, local copies, waits for them, and re-layouts  2.09 us

profile of v4, /device:TPU:1, one launch (start us, length us, event | category | flops | bytes accessed | tf_op | source)
XLA Modules:
  0.0 90.5 jit_solution(4618076765498252732)
XLA Ops:
  0.0 88.4 %shard_map.100 = bf16[192,2048]{1,0:T(8,128)(2,1)} custom-call(bf16[192,2048]{1,0:T(8,128)(2,1)} %res_h.1, bf16[768,256]{1,0:T(8,128)(2,1)} %q_h.1, bf16[64,768]{1,0:T(8,128)(2,1)} %bitcast.4, bf16[64,768]{1,0:T(8,128)(2,1)} %bitcast.5, f32[4]{0:T(128)} %sink_s.1, bf16[1024,2048]{1,0:T(8,128)(2,1)} %wo_h.1, f32[1,2048]{1,0:T(1,128)} %bitcast.7, ...), custom_call_target="tpu_custom_call" | custom-call | tf_op jit(solution)/shard_map/pallas_call | solution.py:414
  88.4 2.1 %copy.12 = bf16[192,2048]{1,0:T(8,128)(2,1)} copy(bf16[192,2048]{1,0:T(8,128)(2,1)} %shard_map.100) | data formatting | bytes 1572864
